TPU v7x, 512 devices: a whole 4x4x16 slice. The times are simulated.
512 devices in a mesh: ep: 16 (over y, x), tp: 32 (over z, core).
Axes of the slice: x: 4, y: 4, z: 16, core: 2. Of those that a mesh axis runs over, the one named last changes fastest.
Arguments:
- tokens: bfloat16 [8192, 4096], P('tp', 'ep'), may hold values from -20 to 20
- norm_gain: bfloat16 [4096], P('ep'), may hold values from 0.099609375 to 1.8984375
- expert_ids: int32 [8192, 2], P('tp'), may hold values from 0 to 31, all different within a row; in each aligned block of 256 rows (0 to 255, 256 to 511, ...) at most 32 rows name the same one
- combine_weight: float32 [8192, 2], P('tp'), may hold values from 0.05 to 1
- w_gate: bfloat16 [32, 2048, 4096], P('tp', 'ep'), may hold values from -0.09375 to 0.09375
- w_up: bfloat16 [32, 2048, 4096], P('tp', 'ep'), may hold values from -0.09375 to 0.09375
- w_down: bfloat16 [32, 2048, 4096], P('tp', None, 'ep'), may hold values from -2 to 2
- out_gain: bfloat16 [4096], P('ep'), may hold values from 0.099609375 to 1.8984375
Outputs:
- mixed: bfloat16 [8192, 4096], P('tp', 'ep')
Inputs may be any that keep to these rules, and one draw needn't show every extreme that they name: `expert_ids`: each row names 2 different experts; among the rows of one index of tp no expert is named by more than 32 rows, a bound that some block reaches.
All inputs are finite; a program needn't handle non-finite values.
Results may differ from a plain program's by a relative error of at most 0.007.
Values may be sent and summed in bfloat16 or wider, within the bound.
No kernel may reach another device: no remote copies, remote signals or barrier semaphores. Data moves between devices by JAX's collectives and lax.ppermute only.
A program may use at most 64 MiB of HBM per device.

v0:
```python
import functools

import jax
import jax.numpy as jnp
from jax import lax
from jax.experimental import pallas as pl
from jax.experimental.pallas import tpu as pltpu
from jax.sharding import PartitionSpec as P


SIDE = 4
CLASSES = 4
EXTRA = 16
epsilon = 1e-06


GRANT = 24 * 1024 * 1024


def klass(i):
    return (i % SIDE + 2 * (i // SIDE)) % CLASSES


def moved(i, dy, dx):
    return (i // SIDE + dy) % SIDE * SIDE + (i % SIDE + dx) % SIDE


def shifted(value, dy, dx):
    n = SIDE * SIDE
    return lax.ppermute(value, "ep", [(i, moved(i, dy, dx)) for i in range(n)])


def slots_of(ids, experts):
    tokens = ids.shape[1]
    expert = lax.broadcasted_iota(jnp.int32, (experts, tokens), 0)
    first, second = ids[0:1] == expert, ids[1:2] == expert
    named = jnp.logical_or(first, second)
    before = lax.broadcasted_iota(jnp.int32, (tokens, tokens), 0) < lax.broadcasted_iota(
        jnp.int32, (tokens, tokens), 1
    )
    rank = jnp.dot(
        named.astype(jnp.float32).astype(jnp.bfloat16),
        before.astype(jnp.float32).astype(jnp.bfloat16),
        preferred_element_type=jnp.float32,
    )
    return first, second, jnp.where(named, rank, -1.0)


def dispatch_kernel(ids_ref, x_ref, out_ref, pick_ref, *, experts, capacity):
    tokens = x_ref.shape[0]
    _, _, slot = slots_of(ids_ref[...], experts)
    place = lax.broadcasted_iota(jnp.int32, (capacity, tokens), 0).astype(jnp.float32)
    for e in range(experts):
        pick = (slot[e : e + 1] == place).astype(jnp.float32).astype(jnp.bfloat16)
        pick_ref[e * capacity : (e + 1) * capacity] = pick
    out_ref[...] = jnp.dot(
        pick_ref[...], x_ref[...], preferred_element_type=jnp.float32
    ).astype(jnp.bfloat16)


def prepare_kernel(ids_ref, w_ref, pick_ref, out_ref, *, experts, capacity):
    tokens = ids_ref.shape[1]
    first, second, slot = slots_of(ids_ref[...], experts)
    place = lax.broadcasted_iota(jnp.int32, (capacity, tokens), 0).astype(jnp.float32)
    for k, mine in enumerate((first, second)):
        own = jnp.where(mine, slot, -1.0)
        for e in range(experts):
            pick = (own[e : e + 1] == place).astype(jnp.float32).astype(jnp.bfloat16)
            pick_ref[k, e * capacity : (e + 1) * capacity] = pick
    for k in range(w_ref.shape[0]):
        out_ref[k] = jnp.broadcast_to(w_ref[k : k + 1], out_ref.shape[1:][::-1]).T


def combine_kernel(pick_ref, w_ref, back_ref, moe_ref, sq_ref):
    moe = None
    for k in range(w_ref.shape[0]):
        picked = lax.dot_general(
            pick_ref[k],
            back_ref[...],
            (((0,), (0,)), ((), ())),
            preferred_element_type=jnp.float32,
        )
        term = picked * w_ref[k][:, 0:1]
        moe = term if moe is None else moe + term
    moe_ref[...] = moe
    squares = lax.dot_general(
        jnp.ones((8, moe.shape[1]), jnp.float32),
        moe * moe,
        (((1,), (1,)), ((), ())),
        precision=lax.Precision.HIGHEST,
        preferred_element_type=jnp.float32,
    )
    for i in range(sq_ref.shape[0]):
        sq_ref[i] = squares[0:1]


def spread_kernel(rows_ref, gain_ref, out_ref):
    rows = rows_ref.shape[1]
    gain = jnp.broadcast_to(gain_ref[...].astype(jnp.float32), (EXTRA, rows_ref.shape[2]))
    gain = gain.astype(jnp.bfloat16)
    for i in range(out_ref.shape[0]):
        out_ref[i, 0:rows, :] = rows_ref[klass(i)]
        out_ref[i, rows : rows + EXTRA, :] = gain


def up_kernel(*refs, pieces, width):
    rows_ref = refs[0]
    gates, ups = refs[1 : 1 + pieces], refs[1 + pieces : 1 + 2 * pieces]
    out_ref, normed = refs[1 + 2 * pieces :]
    sources, _, local = rows_ref.shape
    units = gates[0].shape[0]
    rows = normed.shape[0]
    squares = jnp.zeros((rows, local), jnp.float32)
    for j in range(sources):
        part = rows_ref[j, 0:rows, :].astype(jnp.float32)
        squares = squares + part * part
    scale = lax.rsqrt(jnp.sum(squares, axis=1, keepdims=True) / width + epsilon)
    for j in range(sources):
        gain = rows_ref[j, rows : rows + EXTRA, :].astype(jnp.float32)[0:1]
        part = rows_ref[j, 0:rows, :].astype(jnp.float32)
        normed[:, j * local : (j + 1) * local] = (part * scale * gain).astype(jnp.bfloat16)
    for n in range(pieces):
        both = lax.dot_general(
            normed[...],
            jnp.concatenate([gates[n][...], ups[n][...]], axis=0),
            (((1,), (1,)), ((), ())),
            preferred_element_type=jnp.float32,
        )
        gate, up = both[:, :units], both[:, units:]
        hidden = (gate / (1.0 + jnp.exp(-gate)) * up).astype(jnp.bfloat16)
        for p in range(out_ref.shape[0]):
            out_ref[p, :, n * units : (n + 1) * units] = hidden


def down_kernel(idx_ref, hidden_ref, *refs, pieces):
    weights = refs[:pieces]
    outs = refs[pieces : 2 * pieces]
    ordered = refs[2 * pieces]
    units = hidden_ref.shape[2] // pieces
    for p in range(hidden_ref.shape[0]):
        for n in range(pieces):
            at = pl.multiple_of(idx_ref[p * pieces + n] * units, units)
            ordered[:, pl.ds(at, units)] = hidden_ref[p, :, n * units : (n + 1) * units]
    for n in range(pieces):
        outs[n][...] = jnp.dot(
            ordered[...], weights[n][...], preferred_element_type=jnp.float32
        ).astype(jnp.bfloat16)


def gather_kernel(q_ref, *refs):
    out_ref = refs[-1]
    for i, ref in enumerate(refs[:-1]):
        out_ref[q_ref[i]] = ref[...]


def in_vmem(value):
    return pltpu.with_memory_space_constraint(value, pltpu.VMEM)


def body(tokens, norm_gain, expert_ids, combine_weight, w_gate, w_up, w_down, out_gain):
    tok_rows, local = tokens.shape
    n_split = lax.axis_size("ep")
    n_route = lax.axis_size("tp")
    width = local * n_split
    experts = w_gate.shape[0] * n_route
    capacity = 2 * expert_ids.shape[1] * tok_rows // experts
    slots = experts * capacity
    rows = n_route * capacity // CLASSES
    units = w_gate.shape[1]
    hidden_all = units * n_split
    w_gate, w_up, w_down = w_gate[0], w_up[0], w_down[0]
    vmem = pl.BlockSpec(memory_space=pltpu.VMEM)
    ids = expert_ids.T

    buffer = pl.pallas_call(
        functools.partial(dispatch_kernel, experts=experts, capacity=capacity),
        out_shape=pltpu.VMEM((slots, local), jnp.bfloat16),
        in_specs=[vmem, vmem],
        out_specs=vmem,
        scratch_shapes=[pltpu.VMEM((slots, tok_rows), jnp.bfloat16)],
        compiler_params=pltpu.CompilerParams(vmem_limit_bytes=GRANT),
        name="dispatch",
    )(ids, tokens)
    arrived = lax.all_to_all(
        buffer.reshape(experts, capacity, local),
        "tp",
        split_axis=0,
        concat_axis=0,
        tiled=True,
    )

    steps = ((0, 1), (0, -1), (1, 0))
    gates = [w_gate, *(shifted(w_gate, *s) for s in steps)]
    ups = [w_up, *(shifted(w_up, *s) for s in steps)]
    downs = [w_down, *(shifted(w_down, *s) for s in steps)]
    pieces = len(gates)

    picks, weights = pl.pallas_call(
        functools.partial(prepare_kernel, experts=experts, capacity=capacity),
        out_shape=[
            pltpu.VMEM((expert_ids.shape[1], slots, tok_rows), jnp.bfloat16),
            pltpu.VMEM((expert_ids.shape[1], tok_rows, 128), jnp.float32),
        ],
        in_specs=[vmem, vmem],
        out_specs=[vmem, vmem],
        compiler_params=pltpu.CompilerParams(vmem_limit_bytes=GRANT),
        name="prepare",
    )(ids, combine_weight.T)
    operand = pl.pallas_call(
        spread_kernel,
        out_shape=pltpu.VMEM((n_split, rows + EXTRA, local), jnp.bfloat16),
        in_specs=[vmem, vmem],
        out_specs=vmem,
        compiler_params=pltpu.CompilerParams(vmem_limit_bytes=GRANT),
        name="spread",
    )(in_vmem(arrived.reshape(CLASSES, rows, local)), norm_gain[None, :])
    gathered = lax.all_to_all(operand, "ep", split_axis=0, concat_axis=0, tiled=True)

    hidden = pl.pallas_call(
        functools.partial(up_kernel, pieces=pieces, width=width),
        out_shape=pltpu.VMEM((SIDE, rows, pieces * units), jnp.bfloat16),
        in_specs=[vmem] * (1 + 2 * pieces),
        out_specs=vmem,
        scratch_shapes=[pltpu.VMEM((rows, width), jnp.bfloat16)],
        compiler_params=pltpu.CompilerParams(vmem_limit_bytes=GRANT),
        name="gate_up",
    )(in_vmem(gathered), *(in_vmem(w) for w in (*gates, *ups)))

    groups = [[i for i in range(n_split) if klass(i) == q] for q in range(CLASSES)]
    shared = lax.all_to_all(
        hidden, "ep", split_axis=0, concat_axis=0, tiled=True, axis_index_groups=groups
    )
    mine = klass(lax.axis_index("ep"))
    table = jnp.asarray(
        [
            [[i, *(moved(i, -dy, -dx) for dy, dx in steps)] for i in group]
            for group in groups
        ],
        jnp.int32,
    ).reshape(CLASSES, SIDE * pieces)
    order = lax.dynamic_index_in_dim(table, mine, 0, keepdims=False)

    outs = pl.pallas_call(
        functools.partial(down_kernel, pieces=pieces),
        out_shape=[pltpu.VMEM((rows, local), jnp.bfloat16)] * pieces,
        in_specs=[pl.BlockSpec(memory_space=pltpu.SMEM)] + [vmem] * (1 + pieces),
        out_specs=[vmem] * pieces,
        scratch_shapes=[pltpu.VMEM((rows, hidden_all), jnp.bfloat16)],
        compiler_params=pltpu.CompilerParams(vmem_limit_bytes=GRANT),
        name="down",
    )(order, in_vmem(shared), *(in_vmem(w) for w in downs))

    pieces_back = [outs[0], *(shifted(out, -dy, -dx) for out, (dy, dx) in zip(outs[1:], steps))]
    places = jnp.asarray([0, *(dx + 2 * dy for dy, dx in steps)], jnp.int32)
    places = (mine + places) % CLASSES
    returned = pl.pallas_call(
        gather_kernel,
        out_shape=pltpu.VMEM((CLASSES, rows, local), jnp.bfloat16),
        in_specs=[pl.BlockSpec(memory_space=pltpu.SMEM)] + [vmem] * pieces,
        out_specs=vmem,
        compiler_params=pltpu.CompilerParams(vmem_limit_bytes=GRANT),
        name="gather",
    )(places, *(in_vmem(piece) for piece in pieces_back))

    answers = lax.all_to_all(
        returned.reshape(n_route, capacity, local),
        "tp",
        split_axis=0,
        concat_axis=0,
        tiled=True,
    )
    moe, squares = pl.pallas_call(
        combine_kernel,
        out_shape=[
            pltpu.VMEM((tok_rows, local), jnp.float32),
            pltpu.VMEM((n_split, 1, tok_rows), jnp.float32),
        ],
        in_specs=[vmem] * 3,
        out_specs=[vmem] * 2,
        compiler_params=pltpu.CompilerParams(vmem_limit_bytes=GRANT),
        name="combine",
    )(in_vmem(picks), in_vmem(weights), in_vmem(answers.reshape(slots, local)))
    squares = lax.all_to_all(squares, "ep", split_axis=0, concat_axis=0, tiled=True)
    total = jnp.sum(squares, axis=(0, 1))
    mixed = (
        moe
        * lax.rsqrt(total / width + epsilon)[:, None]
        * out_gain.astype(jnp.float32)[None, :]
    )
    return mixed.astype(jnp.bfloat16)


def solution(mesh):
    return jax.shard_map(
        body,
        mesh=mesh,
        in_specs=(
            P("tp", "ep"),
            P("ep"),
            P("tp", None),
            P("tp", None),
            P("tp", "ep", None),
            P("tp", "ep", None),
            P("tp", None, "ep"),
            P("ep"),
        ),
        out_specs=P("tp", "ep"),
        check_vma=False,
    )
```

profile of v0, /device:TPU:1, one launch (start us, length us, event | category | flops | bytes accessed | tf_op | source)
XLA Modules:
  0.0 243.9 jit_solution(13527225984848115117)
XLA Ops:
  0.0 0.9 copy-done.14
  0.9 0.7 copy-done.15
  1.6 1.2 dispatch.1
  2.8 16.7 %all-to-all-start = ((bf16[32,32,256]{2,1,0:T(8,128)(2,1)}), bf16[32,32,256]{2,1,0:T(8,128)(2,1)S(1)}, u32[]{:S(2)}, u32[]{:S(2)}) async-start(bf16[32,32,256]{2,1,0:T(8,128)(2,1)} %bitcast.3), calls=%async_computation | async-start | bytes 1048576 | tf_op jit(solution)/shard_map/all_to_all | solution.py:184
  19.6 3.1 %collective-permute-start = (bf16[128,4096]{1,0:T(8,128)(2,1)}, bf16[128,4096]{1,0:T(8,128)(2,1)}, u32[]{:S(2)}, u32[]{:S(2)}) collective-permute-start(bf16[128,4096]{1,0:T(8,128)(2,1)} %bitcast.13), channel_id=1, source_target_pairs={{0,32},{32,64},{64,96},{96,0},{128,160},{160,192},{192,224},{224,1... | collective-permute-start | bytes 3145736 | tf_op jit(solution)/shard_map/ppermute | solution.py:30
  22.7 0.7 broadcast_in_dim.2.gain_ref
  23.3 29.7 %all-to-all-done = bf16[32,32,256]{2,1,0:T(8,128)(2,1)S(1)} async-done(((bf16[32,32,256]{2,1,0:T(8,128)(2,1)}), bf16[32,32,256]{2,1,0:T(8,128)(2,1)S(1)}, u32[]{:S(2)}, u32[]{:S(2)}) %all-to-all-start) | async-done | bytes 524320 | tf_op jit(solution)/shard_map/all_to_all | solution.py:184
  53.2 1.4 copy-done
  54.6 6.9 %all-to-all-start.1 = ((bf16[16,272,256]{2,1,0:T(8,128)(2,1)}), bf16[16,272,256]{2,1,0:T(8,128)(2,1)S(1)}, u32[]{:S(2)}, u32[]{:S(2)}) async-start(bf16[16,272,256]{2,1,0:T(8,128)(2,1)} %copy-done), calls=%async_computation.1 | async-start | bytes 4456448 | tf_op jit(solution)/shard_map/all_to_all | solution.py:217
  61.5 4.5 %collective-permute-start.1 = (bf16[128,4096]{1,0:T(8,128)(2,1)S(1)}, bf16[128,4096]{1,0:T(8,128)(2,1)S(1)}, u32[]{:S(2)}, u32[]{:S(2)}) collective-permute-start(bf16[128,4096]{1,0:T(8,128)(2,1)S(1)} %bitcast.14), channel_id=1, source_target_pairs={{0,96},{32,0},{64,32},{96,64},{128,224},{160,128},{192,160},{224,1... | collective-permute-start | bytes 3145736 | tf_op jit(solution)/shard_map/ppermute | solution.py:30
  66.0 3.1 %collective-permute-start.2 = (bf16[128,4096]{1,0:T(8,128)(2,1)S(1)}, bf16[128,4096]{1,0:T(8,128)(2,1)S(1)}, u32[]{:S(2)}, u32[]{:S(2)}) collective-permute-start(bf16[128,4096]{1,0:T(8,128)(2,1)S(1)} %bitcast.15), channel_id=1, source_target_pairs={{0,128},{32,160},{64,192},{96,224},{128,256},{160,288},{192,320},{... | collective-permute-start | bytes 3145736 | tf_op jit(solution)/shard_map/ppermute | solution.py:30
  69.1 1.9 collective-permute-start.3
  71.0 4.6 %collective-permute-start.4 = (bf16[128,4096]{1,0:T(8,128)(2,1)}, bf16[128,4096]{1,0:T(8,128)(2,1)S(1)}, u32[]{:S(2)}, u32[]{:S(2)}) collective-permute-start(bf16[128,4096]{1,0:T(8,128)(2,1)} %bitcast.18), channel_id=1, source_target_pairs={{0,96},{32,0},{64,32},{96,64},{128,224},{160,128},{192,160},{224,1... | collective-permute-start | bytes 3145736 | tf_op jit(solution)/shard_map/ppermute | solution.py:30
  75.6 3.1 %collective-permute-start.5 = (bf16[128,4096]{1,0:T(8,128)(2,1)}, bf16[128,4096]{1,0:T(8,128)(2,1)S(1)}, u32[]{:S(2)}, u32[]{:S(2)}) collective-permute-start(bf16[128,4096]{1,0:T(8,128)(2,1)} %bitcast.19), channel_id=1, source_target_pairs={{0,128},{32,160},{64,192},{96,224},{128,256},{160,288},{192,320},{... | collective-permute-start | bytes 3145736 | tf_op jit(solution)/shard_map/ppermute | solution.py:30
  78.7 36.4 %collective-permute-done.1.refs_3_ = bf16[128,4096]{1,0:T(8,128)(2,1)S(1)} collective-permute-done((bf16[128,4096]{1,0:T(8,128)(2,1)S(1)}, bf16[128,4096]{1,0:T(8,128)(2,1)S(1)}, u32[]{:S(2)}, u32[]{:S(2)}) %collective-permute-start.1) | collective-permute-done | bytes 1048608 | tf_op jit(solution)/shard_map/ppermute | solution.py:30
  115.1 1.0 copy-done.3
  116.1 1.9 collective-permute-start.6
  118.1 1.0 copy-done.5
  119.1 4.6 %collective-permute-start.7 = (bf16[2048,256]{1,0:T(8,128)(2,1)}, bf16[2048,256]{1,0:T(8,128)(2,1)}, u32[]{:S(2)}, u32[]{:S(2)}) collective-permute-start(bf16[2048,256]{1,0:T(8,128)(2,1)} %bitcast.22), channel_id=1, source_target_pairs={{0,96},{32,0},{64,32},{96,64},{128,224},{160,128},{192,160},{224,1... | collective-permute-start | bytes 3145736 | tf_op jit(solution)/shard_map/ppermute | solution.py:30
  123.7 1.0 copy-done.7
  124.6 1.9 collective-permute-start.8
  126.6 11.2 %collective-permute-done.4.refs_7_ = bf16[128,4096]{1,0:T(8,128)(2,1)S(1)} collective-permute-done((bf16[128,4096]{1,0:T(8,128)(2,1)}, bf16[128,4096]{1,0:T(8,128)(2,1)S(1)}, u32[]{:S(2)}, u32[]{:S(2)}) %collective-permute-start.4) | collective-permute-done | bytes 1048608 | tf_op jit(solution)/shard_map/ppermute | solution.py:30
  137.7 1.0 copy-done.9
  138.7 1.0 copy-done.11
  139.7 1.2 copy-done.2
  140.9 1.2 copy-done.4
  142.1 1.2 copy-done.6
  143.3 1.2 copy-done.8
  144.6 1.2 copy-done.10
  145.8 1.2 copy-done.12
  147.0 5.0 %gate_up.1 = bf16[4,256,512]{2,1,0:T(8,128)(2,1)} custom-call(bf16[16,272,256]{2,1,0:T(8,128)(2,1)S(1)} %all-to-all-done.1.refs_0_, bf16[128,4096]{1,0:T(8,128)(2,1)S(1)} %bitcast.16, bf16[128,4096]{1,0:T(8,128)(2,1)} %collective-permute-done.refs_2_, bf16[128,4096]{1,0:T(8,128)(2,1)S(1)} %copy-done.4, bf16[128,4096]{1,0:T(8,128)(2,1)S(1)} %copy-done.6, ...), custom_call_target="tpu_custom_call" | custom-call | tf_op jit(solution)/shard_map/gate_up/pallas_call | solution.py:219
  152.0 3.8 %all-to-all-start.2 = ((bf16[4,256,512]{2,1,0:T(8,128)(2,1)}), bf16[4,256,512]{2,1,0:T(8,128)(2,1)S(1)}, u32[]{:S(2)}, u32[]{:S(2)}) async-start(bf16[4,256,512]{2,1,0:T(8,128)(2,1)} %gate_up.1), calls=%async_computation.2 | async-start | bytes 2097152 | tf_op jit(solution)/shard_map/all_to_all | solution.py:230
  155.8 0.7 dynamic-slice_bitcast_fusion.idx_ref
  156.5 3.7 %collective-permute-done.7.refs_2_ = bf16[2048,256]{1,0:T(8,128)(2,1)} collective-permute-done((bf16[2048,256]{1,0:T(8,128)(2,1)}, bf16[2048,256]{1,0:T(8,128)(2,1)}, u32[]{:S(2)}, u32[]{:S(2)}) %collective-permute-start.7) | collective-permute-done | bytes 1048608 | tf_op jit(solution)/shard_map/ppermute | solution.py:30
  160.2 11.3 %all-to-all-done.2.hidden_ref = bf16[4,256,512]{2,1,0:T(8,128)(2,1)S(1)} async-done(((bf16[4,256,512]{2,1,0:T(8,128)(2,1)}), bf16[4,256,512]{2,1,0:T(8,128)(2,1)S(1)}, u32[]{:S(2)}, u32[]{:S(2)}) %all-to-all-start.2) | async-done | bytes 1048608 | tf_op jit(solution)/shard_map/all_to_all | solution.py:230
  171.5 3.4 %down.1 = (bf16[256,256]{1,0:T(8,128)(2,1)S(1)}, bf16[256,256]{1,0:T(8,128)(2,1)S(1)}, bf16[256,256]{1,0:T(8,128)(2,1)S(1)}, bf16[256,256]{1,0:T(8,128)(2,1)S(1)}) custom-call(s32[16]{0:T(128)S(1)} %dynamic-slice_bitcast_fusion.idx_ref, bf16[4,256,512]{2,1,0:T(8,128)(2,1)S(1)} %all-to-all-done.2.hidden_ref, bf16[2048,256]{1,0:T(8,128)(2,1)S(1)} %bitcast.24, ...), custom_call_target="tpu_custom_call" | custom-call | tf_op jit(solution)/shard_map/down/pallas_call | solution.py:243
  174.9 1.9 collective-permute-start.10
  176.9 2.6 %collective-permute-start.11 = (bf16[256,256]{1,0:T(8,128)(2,1)S(1)}, bf16[256,256]{1,0:T(8,128)(2,1)S(1)}, u32[]{:S(2)}, u32[]{:S(2)}) collective-permute-start(bf16[256,256]{1,0:T(8,128)(2,1)S(1)} %get-tuple-element.18), channel_id=1, source_target_pairs={{0,384},{32,416},{64,448},{96,480},{128,0},{160,32},{192,64},{224,... | collective-permute-start | bytes 393224 | tf_op jit(solution)/shard_map/ppermute | solution.py:30
  179.5 5.8 %collective-permute-start.9 = (bf16[256,256]{1,0:T(8,128)(2,1)S(1)}, bf16[256,256]{1,0:T(8,128)(2,1)S(1)}, u32[]{:S(2)}, u32[]{:S(2)}) collective-permute-start(bf16[256,256]{1,0:T(8,128)(2,1)S(1)} %get-tuple-element.16), channel_id=1, source_target_pairs={{0,96},{32,0},{64,32},{96,64},{128,224},{160,128},{192,160},{224,1... | collective-permute-start | bytes 393224 | tf_op jit(solution)/shard_map/ppermute | solution.py:30
  185.3 1.9 collective-permute-done.9.refs_1_
  187.2 1.4 gather.1
  188.5 8.0 %all-to-all-start.3 = ((bf16[32,32,256]{2,1,0:T(8,128)(2,1)}), bf16[32,32,256]{2,1,0:T(8,128)(2,1)S(1)}, u32[]{:S(2)}, u32[]{:S(2)}) async-start(bf16[32,32,256]{2,1,0:T(8,128)(2,1)} %bitcast.8), calls=%async_computation.3 | async-start | bytes 1048576 | tf_op jit(solution)/shard_map/all_to_all | solution.py:265
  196.6 0.3 prepare.1
  197.0 33.1 %all-to-all-done.3 = bf16[32,32,256]{2,1,0:T(8,128)(2,1)S(1)} async-done(((bf16[32,32,256]{2,1,0:T(8,128)(2,1)}), bf16[32,32,256]{2,1,0:T(8,128)(2,1)S(1)}, u32[]{:S(2)}, u32[]{:S(2)}) %all-to-all-start.3) | async-done | bytes 524320 | tf_op jit(solution)/shard_map/all_to_all | solution.py:265
  230.1 1.6 combine.1
  231.7 5.0 %all-to-all-start.4 = ((f32[16,1,256]{2,1,0:T(1,128)}), f32[16,1,256]{2,1,0:T(1,128)S(1)}, u32[]{:S(2)}, u32[]{:S(2)}) async-start(f32[16,1,256]{2,1,0:T(1,128)} %get-tuple-element.20), calls=%async_computation.4 | async-start | bytes 32768 | tf_op jit(solution)/shard_map/all_to_all | solution.py:283
  236.7 6.4 %all-to-all-done.4 = f32[16,1,256]{2,1,0:T(1,128)S(1)} async-done(((f32[16,1,256]{2,1,0:T(1,128)}), f32[16,1,256]{2,1,0:T(1,128)S(1)}, u32[]{:S(2)}, u32[]{:S(2)}) %all-to-all-start.4) | async-done | bytes 16416 | tf_op jit(solution)/shard_map/all_to_all | solution.py:283
  243.2 0.8 multiply_convert_fusion
  (40 shorter events, 0.3 us)
Async XLA Ops:
  0.0 0.9 copy-start.14
  0.9 0.7 copy-start.15
  2.8 50.3 %all-to-all-start = ((bf16[32,32,256]{2,1,0:T(8,128)(2,1)}), bf16[32,32,256]{2,1,0:T(8,128)(2,1)S(1)}, u32[]{:S(2)}, u32[]{:S(2)}) async-start(bf16[32,32,256]{2,1,0:T(8,128)(2,1)} %bitcast.3), calls=%async_computation | async-start | bytes 1048576 | tf_op jit(solution)/shard_map/all_to_all | solution.py:184
  19.6 56.1 %collective-permute-start = (bf16[128,4096]{1,0:T(8,128)(2,1)}, bf16[128,4096]{1,0:T(8,128)(2,1)}, u32[]{:S(2)}, u32[]{:S(2)}) collective-permute-start(bf16[128,4096]{1,0:T(8,128)(2,1)} %bitcast.13), channel_id=1, source_target_pairs={{0,32},{32,64},{64,96},{96,0},{128,160},{160,192},{192,224},{224,1... | collective-permute-start | bytes 3145736 | tf_op jit(solution)/shard_map/ppermute | solution.py:30
  53.2 1.4 copy-start
  54.6 6.9 %copy-start.1 = (bf16[1,128,4096]{2,1,0:T(8,128)(2,1)S(1)}, bf16[1,128,4096]{2,1,0:T(8,128)(2,1)}, u32[]{:S(2)}) copy-start(bf16[1,128,4096]{2,1,0:T(8,128)(2,1)} %param.14) | copy-start | bytes 3145732
  54.6 85.0 %all-to-all-start.1 = ((bf16[16,272,256]{2,1,0:T(8,128)(2,1)}), bf16[16,272,256]{2,1,0:T(8,128)(2,1)S(1)}, u32[]{:S(2)}, u32[]{:S(2)}) async-start(bf16[16,272,256]{2,1,0:T(8,128)(2,1)} %copy-done), calls=%async_computation.1 | async-start | bytes 4456448 | tf_op jit(solution)/shard_map/all_to_all | solution.py:217
  61.5 53.6 %collective-permute-start.1 = (bf16[128,4096]{1,0:T(8,128)(2,1)S(1)}, bf16[128,4096]{1,0:T(8,128)(2,1)S(1)}, u32[]{:S(2)}, u32[]{:S(2)}) collective-permute-start(bf16[128,4096]{1,0:T(8,128)(2,1)S(1)} %bitcast.14), channel_id=1, source_target_pairs={{0,96},{32,0},{64,32},{96,64},{128,224},{160,128},{192,160},{224,1... | collective-permute-start | bytes 3145736 | tf_op jit(solution)/shard_map/ppermute | solution.py:30
  66.0 52.0 %collective-permute-start.2 = (bf16[128,4096]{1,0:T(8,128)(2,1)S(1)}, bf16[128,4096]{1,0:T(8,128)(2,1)S(1)}, u32[]{:S(2)}, u32[]{:S(2)}) collective-permute-start(bf16[128,4096]{1,0:T(8,128)(2,1)S(1)} %bitcast.15), channel_id=1, source_target_pairs={{0,128},{32,160},{64,192},{96,224},{128,256},{160,288},{192,320},{... | collective-permute-start | bytes 3145736 | tf_op jit(solution)/shard_map/ppermute | solution.py:30
  69.1 54.6 %collective-permute-start.3 = (bf16[128,4096]{1,0:T(8,128)(2,1)}, bf16[128,4096]{1,0:T(8,128)(2,1)S(1)}, u32[]{:S(2)}, u32[]{:S(2)}) collective-permute-start(bf16[128,4096]{1,0:T(8,128)(2,1)} %bitcast.17), channel_id=1, source_target_pairs={{0,32},{32,64},{64,96},{96,0},{128,160},{160,192},{192,224},{224,1... | collective-permute-start | bytes 3145736 | tf_op jit(solution)/shard_map/ppermute | solution.py:30
  71.0 66.7 %collective-permute-start.4 = (bf16[128,4096]{1,0:T(8,128)(2,1)}, bf16[128,4096]{1,0:T(8,128)(2,1)S(1)}, u32[]{:S(2)}, u32[]{:S(2)}) collective-permute-start(bf16[128,4096]{1,0:T(8,128)(2,1)} %bitcast.18), channel_id=1, source_target_pairs={{0,96},{32,0},{64,32},{96,64},{128,224},{160,128},{192,160},{224,1... | collective-permute-start | bytes 3145736 | tf_op jit(solution)/shard_map/ppermute | solution.py:30
  75.6 63.1 %collective-permute-start.5 = (bf16[128,4096]{1,0:T(8,128)(2,1)}, bf16[128,4096]{1,0:T(8,128)(2,1)S(1)}, u32[]{:S(2)}, u32[]{:S(2)}) collective-permute-start(bf16[128,4096]{1,0:T(8,128)(2,1)} %bitcast.19), channel_id=1, source_target_pairs={{0,128},{32,160},{64,192},{96,224},{128,256},{160,288},{192,320},{... | collective-permute-start | bytes 3145736 | tf_op jit(solution)/shard_map/ppermute | solution.py:30
  115.1 1.0 copy-start.3
  116.1 40.3 %collective-permute-start.6 = (bf16[2048,256]{1,0:T(8,128)(2,1)}, bf16[2048,256]{1,0:T(8,128)(2,1)}, u32[]{:S(2)}, u32[]{:S(2)}) collective-permute-start(bf16[2048,256]{1,0:T(8,128)(2,1)} %bitcast.21), channel_id=1, source_target_pairs={{0,32},{32,64},{64,96},{96,0},{128,160},{160,192},{192,224},{224,1... | collective-permute-start | bytes 3145736 | tf_op jit(solution)/shard_map/ppermute | solution.py:30
  118.1 1.0 copy-start.5
  119.1 41.1 %collective-permute-start.7 = (bf16[2048,256]{1,0:T(8,128)(2,1)}, bf16[2048,256]{1,0:T(8,128)(2,1)}, u32[]{:S(2)}, u32[]{:S(2)}) collective-permute-start(bf16[2048,256]{1,0:T(8,128)(2,1)} %bitcast.22), channel_id=1, source_target_pairs={{0,96},{32,0},{64,32},{96,64},{128,224},{160,128},{192,160},{224,1... | collective-permute-start | bytes 3145736 | tf_op jit(solution)/shard_map/ppermute | solution.py:30
  123.7 1.0 copy-start.7
  124.6 35.5 %collective-permute-start.8 = (bf16[2048,256]{1,0:T(8,128)(2,1)}, bf16[2048,256]{1,0:T(8,128)(2,1)}, u32[]{:S(2)}, u32[]{:S(2)}) collective-permute-start(bf16[2048,256]{1,0:T(8,128)(2,1)} %bitcast.23), channel_id=1, source_target_pairs={{0,128},{32,160},{64,192},{96,224},{128,256},{160,288},{192,320},{... | collective-permute-start | bytes 3145736 | tf_op jit(solution)/shard_map/ppermute | solution.py:30
  137.7 1.0 copy-start.9
  138.7 1.0 copy-start.11
  139.7 1.2 copy-start.2
  140.9 1.2 copy-start.4
  142.1 1.2 copy-start.6
  143.3 1.2 copy-start.8
  144.6 1.2 copy-start.10
  145.8 1.2 copy-start.12
  152.0 19.5 %copy-start.13 = (bf16[1,2048,256]{2,1,0:T(8,128)(2,1)S(1)}, bf16[1,2048,256]{2,1,0:T(8,128)(2,1)}, u32[]{:S(2)}) copy-start(bf16[1,2048,256]{2,1,0:T(8,128)(2,1)} %param.16) | copy-start | bytes 3145732
  152.0 19.5 %all-to-all-start.2 = ((bf16[4,256,512]{2,1,0:T(8,128)(2,1)}), bf16[4,256,512]{2,1,0:T(8,128)(2,1)S(1)}, u32[]{:S(2)}, u32[]{:S(2)}) async-start(bf16[4,256,512]{2,1,0:T(8,128)(2,1)} %gate_up.1), calls=%async_computation.2 | async-start | bytes 2097152 | tf_op jit(solution)/shard_map/all_to_all | solution.py:230
  156.5 28.8 %copy-start.19 = (s32[4]{0:T(128)S(1)}, s32[4]{0:T(128)}, u32[]{:S(2)}) copy-start(s32[4]{0:T(128)} %constant.61.clone) | copy-start | bytes 52
  156.5 40.1 %copy-start.16 = (s32[256,2]{0,1:T(2,128)S(1)}, s32[256,2]{0,1:T(2,128)}, u32[]{:S(2)}) copy-start(s32[256,2]{0,1:T(2,128)} %param.12) | copy-start | bytes 6148
  156.5 40.1 %copy-start.17 = (f32[256,2]{0,1:T(2,128)S(1)}, f32[256,2]{0,1:T(2,128)}, u32[]{:S(2)}) copy-start(f32[256,2]{0,1:T(2,128)} %param.13) | copy-start | bytes 6148
  174.9 61.8 %copy-start.18 = (bf16[256]{0:T(256)(128)(2,1)S(1)}, bf16[256]{0:T(256)(128)(2,1)}, u32[]{:S(2)}) copy-start(bf16[256]{0:T(256)(128)(2,1)} %param.17) | copy-start | bytes 1540
  174.9 10.4 %collective-permute-start.10 = (bf16[256,256]{1,0:T(8,128)(2,1)S(1)}, bf16[256,256]{1,0:T(8,128)(2,1)S(1)}, u32[]{:S(2)}, u32[]{:S(2)}) collective-permute-start(bf16[256,256]{1,0:T(8,128)(2,1)S(1)} %get-tuple-element.17), channel_id=1, source_target_pairs={{0,32},{32,64},{64,96},{96,0},{128,160},{160,192},{192,224},{224,1... | collective-permute-start | bytes 393224 | tf_op jit(solution)/shard_map/ppermute | solution.py:30
  176.9 8.4 %collective-permute-start.11 = (bf16[256,256]{1,0:T(8,128)(2,1)S(1)}, bf16[256,256]{1,0:T(8,128)(2,1)S(1)}, u32[]{:S(2)}, u32[]{:S(2)}) collective-permute-start(bf16[256,256]{1,0:T(8,128)(2,1)S(1)} %get-tuple-element.18), channel_id=1, source_target_pairs={{0,384},{32,416},{64,448},{96,480},{128,0},{160,32},{192,64},{224,... | collective-permute-start | bytes 393224 | tf_op jit(solution)/shard_map/ppermute | solution.py:30
  179.5 7.7 %collective-permute-start.9 = (bf16[256,256]{1,0:T(8,128)(2,1)S(1)}, bf16[256,256]{1,0:T(8,128)(2,1)S(1)}, u32[]{:S(2)}, u32[]{:S(2)}) collective-permute-start(bf16[256,256]{1,0:T(8,128)(2,1)S(1)} %get-tuple-element.16), channel_id=1, source_target_pairs={{0,96},{32,0},{64,32},{96,64},{128,224},{160,128},{192,160},{224,1... | collective-permute-start | bytes 393224 | tf_op jit(solution)/shard_map/ppermute | solution.py:30
  188.5 41.6 %all-to-all-start.3 = ((bf16[32,32,256]{2,1,0:T(8,128)(2,1)}), bf16[32,32,256]{2,1,0:T(8,128)(2,1)S(1)}, u32[]{:S(2)}, u32[]{:S(2)}) async-start(bf16[32,32,256]{2,1,0:T(8,128)(2,1)} %bitcast.8), calls=%async_computation.3 | async-start | bytes 1048576 | tf_op jit(solution)/shard_map/all_to_all | solution.py:265
  231.7 11.4 %all-to-all-start.4 = ((f32[16,1,256]{2,1,0:T(1,128)}), f32[16,1,256]{2,1,0:T(1,128)S(1)}, u32[]{:S(2)}, u32[]{:S(2)}) async-start(f32[16,1,256]{2,1,0:T(1,128)} %get-tuple-element.20), calls=%async_computation.4 | async-start | bytes 32768 | tf_op jit(solution)/shard_map/all_to_all | solution.py:283
where the time goes:
time: 245 us; the launch traced here: 244 us
  waiting for transfers between devices  134 us (55%)
  starting transfers between devices  79.4 us (32%)
  local copies, waits for them, and re-layouts  16.6 us (7%)
  Pallas kernels  13 us (5%)
    ppermute x12, waiting for transfers between devices, shifted(): return lax.ppermute(value, 'ep', [(i, moved(i, dy, dx)) for i in range(n)])  53.2 us
    ppermute x12, starting transfers between devices, shifted(): return lax.ppermute(value, 'ep', [(i, moved(i, dy, dx)) for i in range(n)])  39 us
    all_to_all x1, waiting for transfers between devices, body(): lax.all_to_all(returned.reshape(n_route, capacity, local), 'tp', split_ax...  33.1 us
    all_to_all x1, waiting for transfers between devices, body(): lax.all_to_all(buffer.reshape(experts, capacity, local), 'tp', split_axis...  29.7 us
    all_to_all x1, starting transfers between devices, body(): lax.all_to_all(buffer.reshape(experts, capacity, local), 'tp', split_axis...  16.7 us
    unnamed x40, local copies, waits for them, and re-layouts  15.2 us
    all_to_all x1, waiting for transfers between devices, body(): lax.all_to_all(hidden, 'ep', split_axis=0, concat_axis=0, tiled=True, axi...  11.3 us
    all_to_all x1, starting transfers between devices, body(): lax.all_to_all(returned.reshape(n_route, capacity, local), 'tp', split_ax...  8.03 us
  transfers between devices with their start and end apart: 17, of which 8 were waited for; matrix products, arithmetic and copies ran while one was open for 1% of the time, Pallas kernels for 2%

commit v1 on v0

--- a/solution.py
+++ b/solution.py
@@ -17,6 +17,10 @@
 GRANT = 24 * 1024 * 1024
 
 
+def turn(i, core):
+    return i if core == 0 else i % SIDE * SIDE + i // SIDE
+
+
 def klass(i):
     return (i % SIDE + 2 * (i // SIDE)) % CLASSES
 
@@ -26,8 +30,23 @@
 
 
 def shifted(value, dy, dx):
-    n = SIDE * SIDE
-    return lax.ppermute(value, "ep", [(i, moved(i, dy, dx)) for i in range(n)])
+    n_route = lax.axis_size("tp")
+    pairs = []
+    for i in range(SIDE * SIDE):
+        for t in range(n_route):
+            to = turn(moved(turn(i, t % 2), dy, dx), t % 2)
+            pairs.append((i * n_route + t, to * n_route + t))
+    return lax.ppermute(value, ("ep", "tp"), pairs)
+
+
+def spread_weights(weight, steps):
+    half = weight.shape[0] // 2
+    return [
+        weight,
+        *(shifted(weight, *s) for s in steps),
+        shifted(weight[:half], -1, 0),
+        shifted(weight[half:], 1, 0),
+    ]
 
 
 def slots_of(ids, experts):
@@ -94,19 +113,19 @@
         sq_ref[i] = squares[0:1]
 
 
-def spread_kernel(rows_ref, gain_ref, out_ref):
+def spread_kernel(q_ref, rows_ref, gain_ref, out_ref):
     rows = rows_ref.shape[1]
     gain = jnp.broadcast_to(gain_ref[...].astype(jnp.float32), (EXTRA, rows_ref.shape[2]))
     gain = gain.astype(jnp.bfloat16)
     for i in range(out_ref.shape[0]):
-        out_ref[i, 0:rows, :] = rows_ref[klass(i)]
+        out_ref[i, 0:rows, :] = rows_ref[q_ref[i]]
         out_ref[i, rows : rows + EXTRA, :] = gain
 
 
-def up_kernel(*refs, pieces, width):
+def up_kernel(*refs, given, width):
     rows_ref = refs[0]
-    gates, ups = refs[1 : 1 + pieces], refs[1 + pieces : 1 + 2 * pieces]
-    out_ref, normed = refs[1 + 2 * pieces :]
+    gates, ups = refs[1 : 1 + given], refs[1 + given : 1 + 2 * given]
+    out_ref, normed = refs[1 + 2 * given :]
     sources, _, local = rows_ref.shape
     units = gates[0].shape[0]
     rows = normed.shape[0]
@@ -119,10 +138,11 @@
         gain = rows_ref[j, rows : rows + EXTRA, :].astype(jnp.float32)[0:1]
         part = rows_ref[j, 0:rows, :].astype(jnp.float32)
         normed[:, j * local : (j + 1) * local] = (part * scale * gain).astype(jnp.bfloat16)
-    for n in range(pieces):
+    for n in range(given - 1):
+        last = given if n == given - 2 else n + 1
         both = lax.dot_general(
             normed[...],
-            jnp.concatenate([gates[n][...], ups[n][...]], axis=0),
+            jnp.concatenate([ref[...] for ref in (*gates[n:last], *ups[n:last])], axis=0),
             (((1,), (1,)), ((), ())),
             preferred_element_type=jnp.float32,
         )
@@ -140,7 +160,14 @@
     for p in range(hidden_ref.shape[0]):
         for n in range(pieces):
             at = pl.multiple_of(idx_ref[p * pieces + n] * units, units)
-            ordered[:, pl.ds(at, units)] = hidden_ref[p, :, n * units : (n + 1) * units]
+            part = hidden_ref[p, :, n * units : (n + 1) * units]
+            if n == pieces - 1:
+                other = hidden_ref[p ^ 2, :, n * units : (n + 1) * units]
+                lane = lax.broadcasted_iota(jnp.int32, part.shape, 1)
+                part = jnp.where(
+                    lane < units // 2, part.astype(jnp.float32), other.astype(jnp.float32)
+                ).astype(jnp.bfloat16)
+            ordered[:, pl.ds(at, units)] = part
     for n in range(pieces):
         outs[n][...] = jnp.dot(
             ordered[...], weights[n][...], preferred_element_type=jnp.float32
@@ -172,9 +199,18 @@
     vmem = pl.BlockSpec(memory_space=pltpu.VMEM)
     ids = expert_ids.T
 
+    smem = pl.BlockSpec(memory_space=pltpu.SMEM)
+    core = lax.axis_index("tp") % 2
+    me = lax.axis_index("ep")
+    place = jnp.where(core == 0, me, turn(me, 1))
+    mine = klass(place)
+    class_of = jnp.asarray(
+        [[klass(turn(i, k)) for i in range(n_split)] for k in range(2)], jnp.int32
+    )
+    class_of = lax.dynamic_index_in_dim(class_of, core, 0, keepdims=False)
     buffer = pl.pallas_call(
         functools.partial(dispatch_kernel, experts=experts, capacity=capacity),
-        out_shape=pltpu.VMEM((slots, local), jnp.bfloat16),
+        out_shape=jax.ShapeDtypeStruct((slots, local), jnp.bfloat16),
         in_specs=[vmem, vmem],
         out_specs=vmem,
         scratch_shapes=[pltpu.VMEM((slots, tok_rows), jnp.bfloat16)],
@@ -189,11 +225,12 @@
         tiled=True,
     )
 
-    steps = ((0, 1), (0, -1), (1, 0))
-    gates = [w_gate, *(shifted(w_gate, *s) for s in steps)]
-    ups = [w_up, *(shifted(w_up, *s) for s in steps)]
-    downs = [w_down, *(shifted(w_down, *s) for s in steps)]
-    pieces = len(gates)
+    steps = ((0, 1), (0, -1))
+    last_steps = ((0, 1), (0, -1), (1, 0))
+    gates = spread_weights(w_gate, steps)
+    ups = spread_weights(w_up, steps)
+    downs = [w_down, *(shifted(w_down, *s) for s in last_steps)]
+    given, pieces = len(gates), len(downs)
 
     picks, weights = pl.pallas_call(
         functools.partial(prepare_kernel, experts=experts, capacity=capacity),
@@ -208,55 +245,83 @@
     )(ids, combine_weight.T)
     operand = pl.pallas_call(
         spread_kernel,
-        out_shape=pltpu.VMEM((n_split, rows + EXTRA, local), jnp.bfloat16),
-        in_specs=[vmem, vmem],
+        out_shape=jax.ShapeDtypeStruct((n_split, rows + EXTRA, local), jnp.bfloat16),
+        in_specs=[smem, vmem, vmem],
         out_specs=vmem,
         compiler_params=pltpu.CompilerParams(vmem_limit_bytes=GRANT),
         name="spread",
-    )(in_vmem(arrived.reshape(CLASSES, rows, local)), norm_gain[None, :])
+    )(class_of, in_vmem(arrived.reshape(CLASSES, rows, local)), norm_gain[None, :])
     gathered = lax.all_to_all(operand, "ep", split_axis=0, concat_axis=0, tiled=True)
 
     hidden = pl.pallas_call(
-        functools.partial(up_kernel, pieces=pieces, width=width),
-        out_shape=pltpu.VMEM((SIDE, rows, pieces * units), jnp.bfloat16),
-        in_specs=[vmem] * (1 + 2 * pieces),
+        functools.partial(up_kernel, given=given, width=width),
+        out_shape=jax.ShapeDtypeStruct((SIDE, rows, pieces * units), jnp.bfloat16),
+        in_specs=[vmem] * (1 + 2 * given),
         out_specs=vmem,
         scratch_shapes=[pltpu.VMEM((rows, width), jnp.bfloat16)],
         compiler_params=pltpu.CompilerParams(vmem_limit_bytes=GRANT),
         name="gate_up",
     )(in_vmem(gathered), *(in_vmem(w) for w in (*gates, *ups)))
 
-    groups = [[i for i in range(n_split) if klass(i) == q] for q in range(CLASSES)]
+    groups = [
+        [
+            [turn(v, k) for v in range(n_split) if klass(v) == q]
+            for q in range(CLASSES)
+        ]
+        for k in range(2)
+    ]
     shared = lax.all_to_all(
-        hidden, "ep", split_axis=0, concat_axis=0, tiled=True, axis_index_groups=groups
-    )
-    mine = klass(lax.axis_index("ep"))
+        hidden,
+        ("ep", "tp"),
+        split_axis=0,
+        concat_axis=0,
+        tiled=True,
+        axis_index_groups=[
+            [i * n_route + t for i in group]
+            for t in range(n_route)
+            for group in groups[t % 2]
+        ],
+    )
     table = jnp.asarray(
         [
-            [[i, *(moved(i, -dy, -dx) for dy, dx in steps)] for i in group]
-            for group in groups
+            [
+                [
+                    turn(v, k)
+                    for i in group
+                    for v in (
+                        turn(i, k),
+                        *(moved(turn(i, k), -dy, -dx) for dy, dx in steps),
+                        moved(turn(i, k), 1, 0),
+                    )
+                ]
+                for group in groups[k]
+            ]
+            for k in range(2)
         ],
         jnp.int32,
-    ).reshape(CLASSES, SIDE * pieces)
-    order = lax.dynamic_index_in_dim(table, mine, 0, keepdims=False)
+    ).reshape(2 * CLASSES, SIDE * pieces)
+    order = lax.dynamic_index_in_dim(table, core * CLASSES + mine, 0, keepdims=False)
 
     outs = pl.pallas_call(
         functools.partial(down_kernel, pieces=pieces),
         out_shape=[pltpu.VMEM((rows, local), jnp.bfloat16)] * pieces,
-        in_specs=[pl.BlockSpec(memory_space=pltpu.SMEM)] + [vmem] * (1 + pieces),
+        in_specs=[smem] + [vmem] * (1 + pieces),
         out_specs=[vmem] * pieces,
         scratch_shapes=[pltpu.VMEM((rows, hidden_all), jnp.bfloat16)],
         compiler_params=pltpu.CompilerParams(vmem_limit_bytes=GRANT),
         name="down",
     )(order, in_vmem(shared), *(in_vmem(w) for w in downs))
 
-    pieces_back = [outs[0], *(shifted(out, -dy, -dx) for out, (dy, dx) in zip(outs[1:], steps))]
-    places = jnp.asarray([0, *(dx + 2 * dy for dy, dx in steps)], jnp.int32)
+    pieces_back = [
+        outs[0],
+        *(shifted(out, -dy, -dx) for out, (dy, dx) in zip(outs[1:], last_steps)),
+    ]
+    places = jnp.asarray([0, *(dx + 2 * dy for dy, dx in last_steps)], jnp.int32)
     places = (mine + places) % CLASSES
     returned = pl.pallas_call(
         gather_kernel,
         out_shape=pltpu.VMEM((CLASSES, rows, local), jnp.bfloat16),
-        in_specs=[pl.BlockSpec(memory_space=pltpu.SMEM)] + [vmem] * pieces,
+        in_specs=[smem] + [vmem] * pieces,
         out_specs=vmem,
         compiler_params=pltpu.CompilerParams(vmem_limit_bytes=GRANT),
         name="gather",

time: 245 us -> 240 us (0.980)
  waiting for transfers between devices: 134 us -> 123 us
  local copies, waits for them, and re-layouts: 16.6 us -> 20.8 us
    ppermute x12 -> x14, waiting for transfers between devices: 53.2 us -> 41.1 us  [shifted(): return lax.ppermute(value, ('ep', 'tp'), pairs)]
    all_to_all x1, waiting for transfers between devices: 11.3 us -> 16.5 us  [body(): lax.all_to_all(hidden, ('ep', 'tp'), split_axis=0, concat_axis=0, tiled=T...]
    all_to_all x1, waiting for transfers between devices: 29.7 us -> 26.1 us  [body(): lax.all_to_all(buffer.reshape(experts, capacity, local), 'tp', split_axis...]
    all_to_all x1, starting transfers between devices: 8.03 us -> 4.94 us  [body(): lax.all_to_all(returned.reshape(n_route, capacity, local), 'tp', split_ax...]
    ppermute x12 -> x14, starting transfers between devices: 39 us -> 41.7 us  [shifted(): return lax.ppermute(value, ('ep', 'tp'), pairs)]
    unnamed x40 -> x50, local copies, waits for them, and re-layouts: 15.2 us -> 17.8 us
  transfers between devices with their start and end apart: 17 -> 19, of which waited for: 8 -> 8; matrix products, arithmetic and copies ran while one was open for 1% -> 1% of each run, Pallas kernels for 2% -> 2%
where the time goes in v1:
time: 240 us; the launch traced here: 239 us
  waiting for transfers between devices  123 us (51%)
  starting transfers between devices  81.1 us (34%)
  local copies, waits for them, and re-layouts  20.8 us (9%)
  Pallas kernels  12.6 us (5%)
    ppermute x14, starting transfers between devices, shifted(): return lax.ppermute(value, ('ep', 'tp'), pairs)  41.7 us
    ppermute x14, waiting for transfers between devices, shifted(): return lax.ppermute(value, ('ep', 'tp'), pairs)  41.1 us
    all_to_all x1, waiting for transfers between devices, body(): lax.all_to_all(returned.reshape(n_route, capacity, local), 'tp', split_ax...  33.2 us
    all_to_all x1, waiting for transfers between devices, body(): lax.all_to_all(buffer.reshape(experts, capacity, local), 'tp', split_axis...  26.1 us
    unnamed x50, local copies, waits for them, and re-layouts  17.8 us
    all_to_all x1, starting transfers between devices, body(): lax.all_to_all(buffer.reshape(experts, capacity, local), 'tp', split_axis...  16.7 us
    all_to_all x1, waiting for transfers between devices, body(): lax.all_to_all(hidden, ('ep', 'tp'), split_axis=0, concat_axis=0, tiled=T...  16.5 us
    all_to_all x1, starting transfers between devices, body(): lax.all_to_all(operand, 'ep', split_axis=0, concat_axis=0, tiled=True)  6.76 us
  transfers between devices with their start and end apart: 19, of which 8 were waited for; matrix products, arithmetic and copies ran while one was open for 1% of the time, Pallas kernels for 2%

profile of v1, /device:TPU:1, one launch (start us, length us, event | category | flops | bytes accessed | tf_op | source)
XLA Modules:
  0.0 239.1 jit_solution(16389844467630493716)
XLA Ops:
  0.0 1.0 copy-done.17
  1.7 1.2 dispatch.1
  2.9 16.7 %all-to-all-start = ((bf16[32,32,256]{2,1,0:T(8,128)(2,1)}), bf16[32,32,256]{2,1,0:T(8,128)(2,1)S(1)}, u32[]{:S(2)}, u32[]{:S(2)}) async-start(bf16[32,32,256]{2,1,0:T(8,128)(2,1)} %bitcast.4), calls=%async_computation | async-start | bytes 1048576 | tf_op jit(solution)/shard_map/all_to_all | solution.py:220
  19.7 1.0 slice_bitcast_fusion.2
  20.7 4.4 %collective-permute-start.2 = (bf16[64,4096]{1,0:T(8,128)(2,1)}, bf16[64,4096]{1,0:T(8,128)(2,1)}, u32[]{:S(2)}, u32[]{:S(2)}) collective-permute-start(bf16[64,4096]{1,0:T(8,128)(2,1)} %get-tuple-element.24), channel_id=1, source_target_pairs={{0,384},{1,97},{2,386},{3,99},{4,388},{5,101},{6,390},{7,103},{8,3... | collective-permute-start | bytes 1572872 | tf_op jit(solution)/shard_map/ppermute | solution.py:39
  25.1 1.9 collective-permute-start.3
  27.1 26.1 %all-to-all-done = bf16[32,32,256]{2,1,0:T(8,128)(2,1)S(1)} async-done(((bf16[32,32,256]{2,1,0:T(8,128)(2,1)}), bf16[32,32,256]{2,1,0:T(8,128)(2,1)S(1)}, u32[]{:S(2)}, u32[]{:S(2)}) %all-to-all-start) | async-done | bytes 524320 | tf_op jit(solution)/shard_map/all_to_all | solution.py:220
  53.9 1.4 copy-done
  55.3 6.8 %all-to-all-start.1 = ((bf16[16,272,256]{2,1,0:T(8,128)(2,1)}), bf16[16,272,256]{2,1,0:T(8,128)(2,1)S(1)}, u32[]{:S(2)}, u32[]{:S(2)}) async-start(bf16[16,272,256]{2,1,0:T(8,128)(2,1)} %copy-done), calls=%async_computation.1 | async-start | bytes 4456448 | tf_op jit(solution)/shard_map/all_to_all | solution.py:254
  62.0 1.3 slice_bitcast_fusion
  63.3 4.5 %collective-permute-start.6 = (bf16[64,4096]{1,0:T(8,128)(2,1)S(1)}, bf16[64,4096]{1,0:T(8,128)(2,1)S(1)}, u32[]{:S(2)}, u32[]{:S(2)}) collective-permute-start(bf16[64,4096]{1,0:T(8,128)(2,1)S(1)} %get-tuple-element.22), channel_id=1, source_target_pairs={{0,384},{1,97},{2,386},{3,99},{4,388},{5,101},{6,390},{7,103},{8,3... | collective-permute-start | bytes 1572872 | tf_op jit(solution)/shard_map/ppermute | solution.py:39
  67.8 3.1 %collective-permute-start = (bf16[128,4096]{1,0:T(8,128)(2,1)S(1)}, bf16[128,4096]{1,0:T(8,128)(2,1)S(1)}, u32[]{:S(2)}, u32[]{:S(2)}) collective-permute-start(bf16[128,4096]{1,0:T(8,128)(2,1)S(1)} %bitcast.21), channel_id=1, source_target_pairs={{0,32},{1,129},{2,34},{3,131},{4,36},{5,133},{6,38},{7,135},{8,40}... | collective-permute-start | bytes 3145736 | tf_op jit(solution)/shard_map/ppermute | solution.py:39
  70.9 3.4 %collective-permute-start.1 = (bf16[128,4096]{1,0:T(8,128)(2,1)S(1)}, bf16[128,4096]{1,0:T(8,128)(2,1)S(1)}, u32[]{:S(2)}, u32[]{:S(2)}) collective-permute-start(bf16[128,4096]{1,0:T(8,128)(2,1)S(1)} %bitcast.22), channel_id=1, source_target_pairs={{0,96},{1,385},{2,98},{3,387},{4,100},{5,389},{6,102},{7,391},{8,1... | collective-permute-start | bytes 3145736 | tf_op jit(solution)/shard_map/ppermute | solution.py:39
  74.3 1.9 collective-permute-start.4
  76.3 4.6 %collective-permute-start.5 = (bf16[128,4096]{1,0:T(8,128)(2,1)}, bf16[128,4096]{1,0:T(8,128)(2,1)S(1)}, u32[]{:S(2)}, u32[]{:S(2)}) collective-permute-start(bf16[128,4096]{1,0:T(8,128)(2,1)} %bitcast.25), channel_id=1, source_target_pairs={{0,96},{1,385},{2,98},{3,387},{4,100},{5,389},{6,102},{7,391},{8,1... | collective-permute-start | bytes 3145736 | tf_op jit(solution)/shard_map/ppermute | solution.py:39
  80.8 23.7 %collective-permute-done.6.refs_9_ = bf16[64,4096]{1,0:T(8,128)(2,1)S(1)} collective-permute-done((bf16[64,4096]{1,0:T(8,128)(2,1)S(1)}, bf16[64,4096]{1,0:T(8,128)(2,1)S(1)}, u32[]{:S(2)}, u32[]{:S(2)}) %collective-permute-start.6) | collective-permute-done | bytes 524320 | tf_op jit(solution)/shard_map/ppermute | solution.py:39
  105.3 1.9 collective-permute-start.7
  107.2 13.5 %collective-permute-done.7.refs_10_ = bf16[64,4096]{1,0:T(8,128)(2,1)S(1)} collective-permute-done((bf16[64,4096]{1,0:T(8,128)(2,1)S(1)}, bf16[64,4096]{1,0:T(8,128)(2,1)S(1)}, u32[]{:S(2)}, u32[]{:S(2)}) %collective-permute-start.7) | collective-permute-done | bytes 524320 | tf_op jit(solution)/shard_map/ppermute | solution.py:39
  121.5 2.3 collective-permute-start.10
  123.9 1.0 copy-done.4
  124.8 2.0 collective-permute-start.8
  126.9 1.0 copy-done.6
  127.9 4.4 %collective-permute-start.9 = (bf16[2048,256]{1,0:T(8,128)(2,1)}, bf16[2048,256]{1,0:T(8,128)(2,1)}, u32[]{:S(2)}, u32[]{:S(2)}) collective-permute-start(bf16[2048,256]{1,0:T(8,128)(2,1)} %bitcast.31), channel_id=1, source_target_pairs={{0,96},{1,385},{2,98},{3,387},{4,100},{5,389},{6,102},{7,391},{8,1... | collective-permute-start | bytes 3145736 | tf_op jit(solution)/shard_map/ppermute | solution.py:39
  132.3 1.0 copy-done.8
  133.4 1.0 copy-done.10
  134.4 1.2 copy-done.2
  135.6 1.2 copy-done.5
  136.8 1.2 copy-done.7
  138.0 1.2 copy-done.9
  139.3 1.2 copy-done.11
  140.5 1.0 copy-done.14
  141.5 1.0 copy-done.16
  142.6 4.0 %gate_up.1 = bf16[4,256,512]{2,1,0:T(8,128)(2,1)S(1)} custom-call(bf16[16,272,256]{2,1,0:T(8,128)(2,1)S(1)} %all-to-all-done.1.refs_0_, bf16[128,4096]{1,0:T(8,128)(2,1)S(1)} %bitcast.23, bf16[128,4096]{1,0:T(8,128)(2,1)S(1)} %copy-done.5, bf16[128,4096]{1,0:T(8,128)(2,1)S(1)} %copy-done.7, bf16[64,4096]{1,0:T(8,128)(2,1)} %collective-permute-done.2.refs_4_, ...), custom_call_target="tpu_custom_call" | custom-call | tf_op jit(solution)/shard_map/gate_up/pallas_call | solution.py:256
  146.5 1.0 copy-done.3
  147.5 4.7 %all-to-all-start.2 = ((bf16[4,256,512]{2,1,0:T(8,128)(2,1)}), bf16[4,256,512]{2,1,0:T(8,128)(2,1)S(1)}, u32[]{:S(2)}, u32[]{:S(2)}) async-start(bf16[4,256,512]{2,1,0:T(8,128)(2,1)} %copy-done.3), calls=%async_computation.2 | async-start | bytes 2097152 | tf_op jit(solution)/shard_map/all_to_all | solution.py:273
  153.0 16.5 %all-to-all-done.2.hidden_ref = bf16[4,256,512]{2,1,0:T(8,128)(2,1)S(1)} async-done(((bf16[4,256,512]{2,1,0:T(8,128)(2,1)}), bf16[4,256,512]{2,1,0:T(8,128)(2,1)S(1)}, u32[]{:S(2)}, u32[]{:S(2)}) %all-to-all-start.2) | async-done | bytes 1048608 | tf_op jit(solution)/shard_map/all_to_all | solution.py:273
  169.5 3.4 %down.1 = (bf16[256,256]{1,0:T(8,128)(2,1)S(1)}, bf16[256,256]{1,0:T(8,128)(2,1)S(1)}, bf16[256,256]{1,0:T(8,128)(2,1)S(1)}, bf16[256,256]{1,0:T(8,128)(2,1)S(1)}) custom-call(s32[16]{0:T(128)S(1)} %dynamic-slice_bitcast_fusion.1.idx_ref, bf16[4,256,512]{2,1,0:T(8,128)(2,1)S(1)} %all-to-all-done.2.hidden_ref, bf16[2048,256]{1,0:T(8,128)(2,1)S(1)} %bitcast.32, ...), custom_call_target="tpu_custom_call" | custom-call | tf_op jit(solution)/shard_map/down/pallas_call | solution.py:305
  172.9 2.7 %collective-permute-start.11 = (bf16[256,256]{1,0:T(8,128)(2,1)S(1)}, bf16[256,256]{1,0:T(8,128)(2,1)S(1)}, u32[]{:S(2)}, u32[]{:S(2)}) collective-permute-start(bf16[256,256]{1,0:T(8,128)(2,1)S(1)} %get-tuple-element.16), channel_id=1, source_target_pairs={{0,96},{1,385},{2,98},{3,387},{4,100},{5,389},{6,102},{7,391},{8,1... | collective-permute-start | bytes 393224 | tf_op jit(solution)/shard_map/ppermute | solution.py:39
  175.7 2.6 %collective-permute-start.12 = (bf16[256,256]{1,0:T(8,128)(2,1)S(1)}, bf16[256,256]{1,0:T(8,128)(2,1)S(1)}, u32[]{:S(2)}, u32[]{:S(2)}) collective-permute-start(bf16[256,256]{1,0:T(8,128)(2,1)S(1)} %get-tuple-element.17), channel_id=1, source_target_pairs={{0,32},{1,129},{2,34},{3,131},{4,36},{5,133},{6,38},{7,135},{8,40}... | collective-permute-start | bytes 393224 | tf_op jit(solution)/shard_map/ppermute | solution.py:39
  178.2 1.9 collective-permute-start.13
  180.2 2.4 %collective-permute-done.12.refs_2_ = bf16[256,256]{1,0:T(8,128)(2,1)S(1)} collective-permute-done((bf16[256,256]{1,0:T(8,128)(2,1)S(1)}, bf16[256,256]{1,0:T(8,128)(2,1)S(1)}, u32[]{:S(2)}, u32[]{:S(2)}) %collective-permute-start.12) | collective-permute-done | bytes 131104 | tf_op jit(solution)/shard_map/ppermute | solution.py:39
  182.6 1.5 collective-permute-done.13.refs_3_
  184.1 1.4 gather.1
  185.5 4.9 %all-to-all-start.3 = ((bf16[32,32,256]{2,1,0:T(8,128)(2,1)}), bf16[32,32,256]{2,1,0:T(8,128)(2,1)S(1)}, u32[]{:S(2)}, u32[]{:S(2)}) async-start(bf16[32,32,256]{2,1,0:T(8,128)(2,1)} %bitcast.13), calls=%async_computation.3 | async-start | bytes 1048576 | tf_op jit(solution)/shard_map/all_to_all | solution.py:330
  190.8 33.2 %all-to-all-done.3 = bf16[32,32,256]{2,1,0:T(8,128)(2,1)S(1)} async-done(((bf16[32,32,256]{2,1,0:T(8,128)(2,1)}), bf16[32,32,256]{2,1,0:T(8,128)(2,1)S(1)}, u32[]{:S(2)}, u32[]{:S(2)}) %all-to-all-start.3) | async-done | bytes 524320 | tf_op jit(solution)/shard_map/all_to_all | solution.py:330
  224.0 1.6 combine.1
  225.6 6.2 %all-to-all-start.4 = ((f32[16,1,256]{2,1,0:T(1,128)}), f32[16,1,256]{2,1,0:T(1,128)S(1)}, u32[]{:S(2)}, u32[]{:S(2)}) async-start(f32[16,1,256]{2,1,0:T(1,128)} %get-tuple-element.20), calls=%async_computation.4 | async-start | bytes 32768 | tf_op jit(solution)/shard_map/all_to_all | solution.py:348
  231.8 6.4 %all-to-all-done.4 = f32[16,1,256]{2,1,0:T(1,128)S(1)} async-done(((f32[16,1,256]{2,1,0:T(1,128)}), f32[16,1,256]{2,1,0:T(1,128)S(1)}, u32[]{:S(2)}, u32[]{:S(2)}) %all-to-all-start.4) | async-done | bytes 16416 | tf_op jit(solution)/shard_map/all_to_all | solution.py:348
  (57 shorter events, 4.9 us)
Async XLA Ops:
  0.0 27.1 %copy-start.23 = (s32[2,16]{1,0:T(2,128)S(1)}, s32[2,16]{1,0:T(2,128)}, u32[]{:S(2)}) copy-start(s32[2,16]{1,0:T(2,128)} %constant.89.clone) | copy-start | bytes 388
  0.0 19.7 %copy-start.1 = (bf16[1,128,4096]{2,1,0:T(8,128)(2,1)S(1)}, bf16[1,128,4096]{2,1,0:T(8,128)(2,1)}, u32[]{:S(2)}) copy-start(bf16[1,128,4096]{2,1,0:T(8,128)(2,1)} %param.15) | copy-start | bytes 3145732
  0.0 1.0 copy-start.17
  1.0 0.7 copy-start.18
  1.7 25.4 %copy-start.21 = (bf16[256]{0:T(256)(128)(2,1)S(1)}, bf16[256]{0:T(256)(128)(2,1)}, u32[]{:S(2)}) copy-start(bf16[256]{0:T(256)(128)(2,1)} %param.12) | copy-start | bytes 1540
  2.9 50.3 %all-to-all-start = ((bf16[32,32,256]{2,1,0:T(8,128)(2,1)}), bf16[32,32,256]{2,1,0:T(8,128)(2,1)S(1)}, u32[]{:S(2)}, u32[]{:S(2)}) async-start(bf16[32,32,256]{2,1,0:T(8,128)(2,1)} %bitcast.4), calls=%async_computation | async-start | bytes 1048576 | tf_op jit(solution)/shard_map/all_to_all | solution.py:220
  20.7 53.6 %collective-permute-start.2 = (bf16[64,4096]{1,0:T(8,128)(2,1)}, bf16[64,4096]{1,0:T(8,128)(2,1)}, u32[]{:S(2)}, u32[]{:S(2)}) collective-permute-start(bf16[64,4096]{1,0:T(8,128)(2,1)} %get-tuple-element.24), channel_id=1, source_target_pairs={{0,384},{1,97},{2,386},{3,99},{4,388},{5,101},{6,390},{7,103},{8,3... | collective-permute-start | bytes 1572872 | tf_op jit(solution)/shard_map/ppermute | solution.py:39
  25.1 51.2 %collective-permute-start.3 = (bf16[64,4096]{1,0:T(8,128)(2,1)}, bf16[64,4096]{1,0:T(8,128)(2,1)}, u32[]{:S(2)}, u32[]{:S(2)}) collective-permute-start(bf16[64,4096]{1,0:T(8,128)(2,1)} %get-tuple-element.23), channel_id=1, source_target_pairs={{0,128},{1,33},{2,130},{3,35},{4,132},{5,37},{6,134},{7,39},{8,136... | collective-permute-start | bytes 1572872 | tf_op jit(solution)/shard_map/ppermute | solution.py:39
  53.9 1.4 copy-start
  55.3 79.1 %all-to-all-start.1 = ((bf16[16,272,256]{2,1,0:T(8,128)(2,1)}), bf16[16,272,256]{2,1,0:T(8,128)(2,1)S(1)}, u32[]{:S(2)}, u32[]{:S(2)}) async-start(bf16[16,272,256]{2,1,0:T(8,128)(2,1)} %copy-done), calls=%async_computation.1 | async-start | bytes 4456448 | tf_op jit(solution)/shard_map/all_to_all | solution.py:254
  63.3 41.2 %collective-permute-start.6 = (bf16[64,4096]{1,0:T(8,128)(2,1)S(1)}, bf16[64,4096]{1,0:T(8,128)(2,1)S(1)}, u32[]{:S(2)}, u32[]{:S(2)}) collective-permute-start(bf16[64,4096]{1,0:T(8,128)(2,1)S(1)} %get-tuple-element.22), channel_id=1, source_target_pairs={{0,384},{1,97},{2,386},{3,99},{4,388},{5,101},{6,390},{7,103},{8,3... | collective-permute-start | bytes 1572872 | tf_op jit(solution)/shard_map/ppermute | solution.py:39
  67.8 56.0 %collective-permute-start = (bf16[128,4096]{1,0:T(8,128)(2,1)S(1)}, bf16[128,4096]{1,0:T(8,128)(2,1)S(1)}, u32[]{:S(2)}, u32[]{:S(2)}) collective-permute-start(bf16[128,4096]{1,0:T(8,128)(2,1)S(1)} %bitcast.21), channel_id=1, source_target_pairs={{0,32},{1,129},{2,34},{3,131},{4,36},{5,133},{6,38},{7,135},{8,40}... | collective-permute-start | bytes 3145736 | tf_op jit(solution)/shard_map/ppermute | solution.py:39
  70.9 56.0 %collective-permute-start.1 = (bf16[128,4096]{1,0:T(8,128)(2,1)S(1)}, bf16[128,4096]{1,0:T(8,128)(2,1)S(1)}, u32[]{:S(2)}, u32[]{:S(2)}) collective-permute-start(bf16[128,4096]{1,0:T(8,128)(2,1)S(1)} %bitcast.22), channel_id=1, source_target_pairs={{0,96},{1,385},{2,98},{3,387},{4,100},{5,389},{6,102},{7,391},{8,1... | collective-permute-start | bytes 3145736 | tf_op jit(solution)/shard_map/ppermute | solution.py:39
  74.3 58.0 %collective-permute-start.4 = (bf16[128,4096]{1,0:T(8,128)(2,1)}, bf16[128,4096]{1,0:T(8,128)(2,1)S(1)}, u32[]{:S(2)}, u32[]{:S(2)}) collective-permute-start(bf16[128,4096]{1,0:T(8,128)(2,1)} %bitcast.24), channel_id=1, source_target_pairs={{0,32},{1,129},{2,34},{3,131},{4,36},{5,133},{6,38},{7,135},{8,40}... | collective-permute-start | bytes 3145736 | tf_op jit(solution)/shard_map/ppermute | solution.py:39
  76.3 57.1 %collective-permute-start.5 = (bf16[128,4096]{1,0:T(8,128)(2,1)}, bf16[128,4096]{1,0:T(8,128)(2,1)S(1)}, u32[]{:S(2)}, u32[]{:S(2)}) collective-permute-start(bf16[128,4096]{1,0:T(8,128)(2,1)} %bitcast.25), channel_id=1, source_target_pairs={{0,96},{1,385},{2,98},{3,387},{4,100},{5,389},{6,102},{7,391},{8,1... | collective-permute-start | bytes 3145736 | tf_op jit(solution)/shard_map/ppermute | solution.py:39
  104.5 0.8 copy-start.13
  105.3 15.4 %collective-permute-start.7 = (bf16[64,4096]{1,0:T(8,128)(2,1)S(1)}, bf16[64,4096]{1,0:T(8,128)(2,1)S(1)}, u32[]{:S(2)}, u32[]{:S(2)}) collective-permute-start(bf16[64,4096]{1,0:T(8,128)(2,1)S(1)} %get-tuple-element.21), channel_id=1, source_target_pairs={{0,128},{1,33},{2,130},{3,35},{4,132},{5,37},{6,134},{7,39},{8,136... | collective-permute-start | bytes 1572872 | tf_op jit(solution)/shard_map/ppermute | solution.py:39
  120.7 0.8 copy-start.15
  121.5 31.4 %collective-permute-start.10 = (bf16[2048,256]{1,0:T(8,128)(2,1)}, bf16[2048,256]{1,0:T(8,128)(2,1)}, u32[]{:S(2)}, u32[]{:S(2)}) collective-permute-start(bf16[2048,256]{1,0:T(8,128)(2,1)} %bitcast.29), channel_id=1, source_target_pairs={{0,128},{1,33},{2,130},{3,35},{4,132},{5,37},{6,134},{7,39},{8,136... | collective-permute-start | bytes 3145736 | tf_op jit(solution)/shard_map/ppermute | solution.py:39
  123.9 1.0 copy-start.4
  124.8 28.1 %collective-permute-start.8 = (bf16[2048,256]{1,0:T(8,128)(2,1)}, bf16[2048,256]{1,0:T(8,128)(2,1)}, u32[]{:S(2)}, u32[]{:S(2)}) collective-permute-start(bf16[2048,256]{1,0:T(8,128)(2,1)} %bitcast.30), channel_id=1, source_target_pairs={{0,32},{1,129},{2,34},{3,131},{4,36},{5,133},{6,38},{7,135},{8,40}... | collective-permute-start | bytes 3145736 | tf_op jit(solution)/shard_map/ppermute | solution.py:39
  126.9 1.0 copy-start.6
  127.9 25.1 %collective-permute-start.9 = (bf16[2048,256]{1,0:T(8,128)(2,1)}, bf16[2048,256]{1,0:T(8,128)(2,1)}, u32[]{:S(2)}, u32[]{:S(2)}) collective-permute-start(bf16[2048,256]{1,0:T(8,128)(2,1)} %bitcast.31), channel_id=1, source_target_pairs={{0,96},{1,385},{2,98},{3,387},{4,100},{5,389},{6,102},{7,391},{8,1... | collective-permute-start | bytes 3145736 | tf_op jit(solution)/shard_map/ppermute | solution.py:39
  132.3 1.1 copy-start.8
  133.4 1.0 copy-start.10
  134.4 1.2 copy-start.2
  135.6 1.2 copy-start.5
  136.8 1.2 copy-start.7
  138.0 1.2 copy-start.9
  139.3 1.2 copy-start.11
  140.5 1.0 copy-start.14
  141.5 1.0 copy-start.16
  146.5 1.0 copy-start.3
  147.5 22.0 %copy-start.12 = (bf16[1,2048,256]{2,1,0:T(8,128)(2,1)S(1)}, bf16[1,2048,256]{2,1,0:T(8,128)(2,1)}, u32[]{:S(2)}) copy-start(bf16[1,2048,256]{2,1,0:T(8,128)(2,1)} %param.17) | copy-start | bytes 3145732
  147.5 22.0 %all-to-all-start.2 = ((bf16[4,256,512]{2,1,0:T(8,128)(2,1)}), bf16[4,256,512]{2,1,0:T(8,128)(2,1)S(1)}, u32[]{:S(2)}, u32[]{:S(2)}) async-start(bf16[4,256,512]{2,1,0:T(8,128)(2,1)} %copy-done.3), calls=%async_computation.2 | async-start | bytes 2097152 | tf_op jit(solution)/shard_map/all_to_all | solution.py:273
  152.9 27.3 %copy-start.24 = (s32[4]{0:T(128)S(1)}, s32[4]{0:T(128)}, u32[]{:S(2)}) copy-start(s32[4]{0:T(128)} %constant.91.clone) | copy-start | bytes 52
  152.9 37.5 %copy-start.19 = (s32[256,2]{0,1:T(2,128)S(1)}, s32[256,2]{0,1:T(2,128)}, u32[]{:S(2)}) copy-start(s32[256,2]{0,1:T(2,128)} %param.13) | copy-start | bytes 6148
  152.9 37.5 %copy-start.20 = (f32[256,2]{0,1:T(2,128)S(1)}, f32[256,2]{0,1:T(2,128)}, u32[]{:S(2)}) copy-start(f32[256,2]{0,1:T(2,128)} %param.14) | copy-start | bytes 6148
  172.9 58.9 %copy-start.22 = (bf16[256]{0:T(256)(128)(2,1)S(1)}, bf16[256]{0:T(256)(128)(2,1)}, u32[]{:S(2)}) copy-start(bf16[256]{0:T(256)(128)(2,1)} %param.18) | copy-start | bytes 1540
  172.9 7.3 %collective-permute-start.11 = (bf16[256,256]{1,0:T(8,128)(2,1)S(1)}, bf16[256,256]{1,0:T(8,128)(2,1)S(1)}, u32[]{:S(2)}, u32[]{:S(2)}) collective-permute-start(bf16[256,256]{1,0:T(8,128)(2,1)S(1)} %get-tuple-element.16), channel_id=1, source_target_pairs={{0,96},{1,385},{2,98},{3,387},{4,100},{5,389},{6,102},{7,391},{8,1... | collective-permute-start | bytes 393224 | tf_op jit(solution)/shard_map/ppermute | solution.py:39
  175.7 6.9 %collective-permute-start.12 = (bf16[256,256]{1,0:T(8,128)(2,1)S(1)}, bf16[256,256]{1,0:T(8,128)(2,1)S(1)}, u32[]{:S(2)}, u32[]{:S(2)}) collective-permute-start(bf16[256,256]{1,0:T(8,128)(2,1)S(1)} %get-tuple-element.17), channel_id=1, source_target_pairs={{0,32},{1,129},{2,34},{3,131},{4,36},{5,133},{6,38},{7,135},{8,40}... | collective-permute-start | bytes 393224 | tf_op jit(solution)/shard_map/ppermute | solution.py:39
  178.2 5.9 %collective-permute-start.13 = (bf16[256,256]{1,0:T(8,128)(2,1)S(1)}, bf16[256,256]{1,0:T(8,128)(2,1)S(1)}, u32[]{:S(2)}, u32[]{:S(2)}) collective-permute-start(bf16[256,256]{1,0:T(8,128)(2,1)S(1)} %get-tuple-element.18), channel_id=1, source_target_pairs={{0,384},{1,97},{2,386},{3,99},{4,388},{5,101},{6,390},{7,103},{8,3... | collective-permute-start | bytes 393224 | tf_op jit(solution)/shard_map/ppermute | solution.py:39
  185.5 38.5 %all-to-all-start.3 = ((bf16[32,32,256]{2,1,0:T(8,128)(2,1)}), bf16[32,32,256]{2,1,0:T(8,128)(2,1)S(1)}, u32[]{:S(2)}, u32[]{:S(2)}) async-start(bf16[32,32,256]{2,1,0:T(8,128)(2,1)} %bitcast.13), calls=%async_computation.3 | async-start | bytes 1048576 | tf_op jit(solution)/shard_map/all_to_all | solution.py:330
  225.6 12.7 %all-to-all-start.4 = ((f32[16,1,256]{2,1,0:T(1,128)}), f32[16,1,256]{2,1,0:T(1,128)S(1)}, u32[]{:S(2)}, u32[]{:S(2)}) async-start(f32[16,1,256]{2,1,0:T(1,128)} %get-tuple-element.20), calls=%async_computation.4 | async-start | bytes 32768 | tf_op jit(solution)/shard_map/all_to_all | solution.py:348

commit v2 on v1

--- a/solution.py
+++ b/solution.py
@@ -78,37 +78,32 @@
 
 
 def prepare_kernel(ids_ref, w_ref, pick_ref, out_ref, *, experts, capacity):
-    tokens = ids_ref.shape[1]
     first, second, slot = slots_of(ids_ref[...], experts)
-    place = lax.broadcasted_iota(jnp.int32, (capacity, tokens), 0).astype(jnp.float32)
+    tall = out_ref.shape[1:][::-1]
+    base = lax.broadcasted_iota(jnp.int32, slot.shape, 0).astype(jnp.float32) * capacity
+    place = lax.broadcasted_iota(jnp.int32, pick_ref.shape[1:], 1).astype(jnp.float32)
     for k, mine in enumerate((first, second)):
-        own = jnp.where(mine, slot, -1.0)
-        for e in range(experts):
-            pick = (own[e : e + 1] == place).astype(jnp.float32).astype(jnp.bfloat16)
-            pick_ref[k, e * capacity : (e + 1) * capacity] = pick
+        target = jnp.sum(jnp.where(mine, base + slot, 0.0), axis=0, keepdims=True)
+        target = jnp.broadcast_to(target, tall).T[:, 0:1]
+        pick_ref[k] = (place == target).astype(jnp.float32).astype(jnp.bfloat16)
     for k in range(w_ref.shape[0]):
-        out_ref[k] = jnp.broadcast_to(w_ref[k : k + 1], out_ref.shape[1:][::-1]).T
+        out_ref[k] = jnp.broadcast_to(w_ref[k : k + 1], tall).T
 
 
 def combine_kernel(pick_ref, w_ref, back_ref, moe_ref, sq_ref):
+    routes, tokens, slots = pick_ref.shape
+    picked = jnp.dot(
+        pick_ref[...].reshape(routes * tokens, slots),
+        back_ref[...],
+        preferred_element_type=jnp.float32,
+    )
     moe = None
-    for k in range(w_ref.shape[0]):
-        picked = lax.dot_general(
-            pick_ref[k],
-            back_ref[...],
-            (((0,), (0,)), ((), ())),
-            preferred_element_type=jnp.float32,
-        )
-        term = picked * w_ref[k][:, 0:1]
+    for k in range(routes):
+        term = picked[k * tokens : (k + 1) * tokens] * w_ref[k][:, 0:1]
         moe = term if moe is None else moe + term
     moe_ref[...] = moe
-    squares = lax.dot_general(
-        jnp.ones((8, moe.shape[1]), jnp.float32),
-        moe * moe,
-        (((1,), (1,)), ((), ())),
-        precision=lax.Precision.HIGHEST,
-        preferred_element_type=jnp.float32,
-    )
+    squares = jnp.sum(moe * moe, axis=1, keepdims=True)
+    squares = jnp.broadcast_to(squares, (tokens, 128)).T
     for i in range(sq_ref.shape[0]):
         sq_ref[i] = squares[0:1]
 
@@ -180,6 +175,10 @@
         out_ref[q_ref[i]] = ref[...]
 
 
+def in_hbm(value):
+    return pltpu.with_memory_space_constraint(value, pltpu.HBM)
+
+
 def in_vmem(value):
     return pltpu.with_memory_space_constraint(value, pltpu.VMEM)
 
@@ -216,7 +215,7 @@
         scratch_shapes=[pltpu.VMEM((slots, tok_rows), jnp.bfloat16)],
         compiler_params=pltpu.CompilerParams(vmem_limit_bytes=GRANT),
         name="dispatch",
-    )(ids, tokens)
+    )(in_hbm(ids), in_hbm(tokens))
     arrived = lax.all_to_all(
         buffer.reshape(experts, capacity, local),
         "tp",
@@ -235,7 +234,7 @@
     picks, weights = pl.pallas_call(
         functools.partial(prepare_kernel, experts=experts, capacity=capacity),
         out_shape=[
-            pltpu.VMEM((expert_ids.shape[1], slots, tok_rows), jnp.bfloat16),
+            pltpu.VMEM((expert_ids.shape[1], tok_rows, slots), jnp.bfloat16),
             pltpu.VMEM((expert_ids.shape[1], tok_rows, 128), jnp.float32),
         ],
         in_specs=[vmem, vmem],
@@ -255,7 +254,7 @@
 
     hidden = pl.pallas_call(
         functools.partial(up_kernel, given=given, width=width),
-        out_shape=jax.ShapeDtypeStruct((SIDE, rows, pieces * units), jnp.bfloat16),
+        out_shape=pltpu.HBM((SIDE, rows, pieces * units), jnp.bfloat16),
         in_specs=[vmem] * (1 + 2 * given),
         out_specs=vmem,
         scratch_shapes=[pltpu.VMEM((rows, width), jnp.bfloat16)],

time: 240 us -> 239 us (level)
  local copies, waits for them, and re-layouts: 20.8 us -> 18.2 us
    unnamed x50 -> x44, local copies, waits for them, and re-layouts: 17.8 us -> 15.1 us
  transfers between devices with their start and end apart: 19 -> 19, of which waited for: 8 -> 8; matrix products, arithmetic and copies ran while one was open for 1% -> 1% of each run, Pallas kernels for 2% -> 3%
where the time goes in v2:
time: 239 us; the launch traced here: 238 us
  waiting for transfers between devices  123 us (51%)
  starting transfers between devices  81.1 us (34%)
  local copies, waits for them, and re-layouts  18.2 us (8%)
  Pallas kernels  14.4 us (6%)
    ppermute x14, starting transfers between devices, shifted(): return lax.ppermute(value, ('ep', 'tp'), pairs)  41.7 us
    ppermute x14, waiting for transfers between devices, shifted(): return lax.ppermute(value, ('ep', 'tp'), pairs)  41.1 us
    all_to_all x1, waiting for transfers between devices, body(): lax.all_to_all(returned.reshape(n_route, capacity, local), 'tp', split_ax...  33 us
    all_to_all x1, waiting for transfers between devices, body(): lax.all_to_all(buffer.reshape(experts, capacity, local), 'tp', split_axis...  26.1 us
    all_to_all x1, starting transfers between devices, body(): lax.all_to_all(buffer.reshape(experts, capacity, local), 'tp', split_axis...  16.7 us
    all_to_all x1, waiting for transfers between devices, body(): lax.all_to_all(hidden, ('ep', 'tp'), split_axis=0, concat_axis=0, tiled=T...  16.5 us
    unnamed x44, local copies, waits for them, and re-layouts  15.1 us
    all_to_all x1, starting transfers between devices, body(): lax.all_to_all(operand, 'ep', split_axis=0, concat_axis=0, tiled=True)  6.75 us
  transfers between devices with their start and end apart: 19, of which 8 were waited for; matrix products, arithmetic and copies ran while one was open for 1% of the time, Pallas kernels for 3%

profile of v2, /device:TPU:1, one launch (start us, length us, event | category | flops | bytes accessed | tf_op | source)
XLA Modules:
  0.0 238.0 jit_solution(11542245162679147137)
XLA Ops:
  0.0 2.3 dispatch.1
  2.3 16.7 %all-to-all-start = ((bf16[32,32,256]{2,1,0:T(8,128)(2,1)}), bf16[32,32,256]{2,1,0:T(8,128)(2,1)S(1)}, u32[]{:S(2)}, u32[]{:S(2)}) async-start(bf16[32,32,256]{2,1,0:T(8,128)(2,1)} %bitcast.4), calls=%async_computation | async-start | bytes 1048576 | tf_op jit(solution)/shard_map/all_to_all | solution.py:219
  19.0 1.1 slice_bitcast_fusion.2
  20.1 4.4 %collective-permute-start.2 = (bf16[64,4096]{1,0:T(8,128)(2,1)}, bf16[64,4096]{1,0:T(8,128)(2,1)}, u32[]{:S(2)}, u32[]{:S(2)}) collective-permute-start(bf16[64,4096]{1,0:T(8,128)(2,1)} %get-tuple-element.24), channel_id=1, source_target_pairs={{0,384},{1,97},{2,386},{3,99},{4,388},{5,101},{6,390},{7,103},{8,3... | collective-permute-start | bytes 1572872 | tf_op jit(solution)/shard_map/ppermute | solution.py:39
  24.5 1.9 collective-permute-start.3
  26.5 26.1 %all-to-all-done = bf16[32,32,256]{2,1,0:T(8,128)(2,1)S(1)} async-done(((bf16[32,32,256]{2,1,0:T(8,128)(2,1)}), bf16[32,32,256]{2,1,0:T(8,128)(2,1)S(1)}, u32[]{:S(2)}, u32[]{:S(2)}) %all-to-all-start) | async-done | bytes 524320 | tf_op jit(solution)/shard_map/all_to_all | solution.py:219
  53.2 1.4 copy-done
  54.6 6.7 %all-to-all-start.1 = ((bf16[16,272,256]{2,1,0:T(8,128)(2,1)}), bf16[16,272,256]{2,1,0:T(8,128)(2,1)S(1)}, u32[]{:S(2)}, u32[]{:S(2)}) async-start(bf16[16,272,256]{2,1,0:T(8,128)(2,1)} %copy-done), calls=%async_computation.1 | async-start | bytes 4456448 | tf_op jit(solution)/shard_map/all_to_all | solution.py:253
  61.4 1.3 slice_bitcast_fusion
  62.6 4.5 %collective-permute-start.6 = (bf16[64,4096]{1,0:T(8,128)(2,1)S(1)}, bf16[64,4096]{1,0:T(8,128)(2,1)S(1)}, u32[]{:S(2)}, u32[]{:S(2)}) collective-permute-start(bf16[64,4096]{1,0:T(8,128)(2,1)S(1)} %get-tuple-element.22), channel_id=1, source_target_pairs={{0,384},{1,97},{2,386},{3,99},{4,388},{5,101},{6,390},{7,103},{8,3... | collective-permute-start | bytes 1572872 | tf_op jit(solution)/shard_map/ppermute | solution.py:39
  67.1 3.1 %collective-permute-start = (bf16[128,4096]{1,0:T(8,128)(2,1)S(1)}, bf16[128,4096]{1,0:T(8,128)(2,1)S(1)}, u32[]{:S(2)}, u32[]{:S(2)}) collective-permute-start(bf16[128,4096]{1,0:T(8,128)(2,1)S(1)} %bitcast.21), channel_id=1, source_target_pairs={{0,32},{1,129},{2,34},{3,131},{4,36},{5,133},{6,38},{7,135},{8,40}... | collective-permute-start | bytes 3145736 | tf_op jit(solution)/shard_map/ppermute | solution.py:39
  70.2 3.4 %collective-permute-start.1 = (bf16[128,4096]{1,0:T(8,128)(2,1)S(1)}, bf16[128,4096]{1,0:T(8,128)(2,1)S(1)}, u32[]{:S(2)}, u32[]{:S(2)}) collective-permute-start(bf16[128,4096]{1,0:T(8,128)(2,1)S(1)} %bitcast.22), channel_id=1, source_target_pairs={{0,96},{1,385},{2,98},{3,387},{4,100},{5,389},{6,102},{7,391},{8,1... | collective-permute-start | bytes 3145736 | tf_op jit(solution)/shard_map/ppermute | solution.py:39
  73.7 1.9 collective-permute-start.4
  75.6 4.6 %collective-permute-start.5 = (bf16[128,4096]{1,0:T(8,128)(2,1)}, bf16[128,4096]{1,0:T(8,128)(2,1)S(1)}, u32[]{:S(2)}, u32[]{:S(2)}) collective-permute-start(bf16[128,4096]{1,0:T(8,128)(2,1)} %bitcast.25), channel_id=1, source_target_pairs={{0,96},{1,385},{2,98},{3,387},{4,100},{5,389},{6,102},{7,391},{8,1... | collective-permute-start | bytes 3145736 | tf_op jit(solution)/shard_map/ppermute | solution.py:39
  80.2 23.7 %collective-permute-done.6.refs_9_ = bf16[64,4096]{1,0:T(8,128)(2,1)S(1)} collective-permute-done((bf16[64,4096]{1,0:T(8,128)(2,1)S(1)}, bf16[64,4096]{1,0:T(8,128)(2,1)S(1)}, u32[]{:S(2)}, u32[]{:S(2)}) %collective-permute-start.6) | collective-permute-done | bytes 524320 | tf_op jit(solution)/shard_map/ppermute | solution.py:39
  103.8 0.8 copy-done.12
  104.6 1.9 collective-permute-start.7
  106.6 13.5 %collective-permute-done.7.refs_10_ = bf16[64,4096]{1,0:T(8,128)(2,1)S(1)} collective-permute-done((bf16[64,4096]{1,0:T(8,128)(2,1)S(1)}, bf16[64,4096]{1,0:T(8,128)(2,1)S(1)}, u32[]{:S(2)}, u32[]{:S(2)}) %collective-permute-start.7) | collective-permute-done | bytes 524320 | tf_op jit(solution)/shard_map/ppermute | solution.py:39
  120.0 0.8 copy-done.14
  120.8 2.3 collective-permute-start.10
  123.2 1.0 copy-done.3
  124.2 2.0 collective-permute-start.8
  126.2 1.0 copy-done.5
  127.2 4.4 %collective-permute-start.9 = (bf16[2048,256]{1,0:T(8,128)(2,1)}, bf16[2048,256]{1,0:T(8,128)(2,1)}, u32[]{:S(2)}, u32[]{:S(2)}) collective-permute-start(bf16[2048,256]{1,0:T(8,128)(2,1)} %bitcast.31), channel_id=1, source_target_pairs={{0,96},{1,385},{2,98},{3,387},{4,100},{5,389},{6,102},{7,391},{8,1... | collective-permute-start | bytes 3145736 | tf_op jit(solution)/shard_map/ppermute | solution.py:39
  131.7 1.0 copy-done.7
  132.7 1.0 copy-done.9
  133.7 1.2 copy-done.2
  134.9 1.2 copy-done.4
  136.1 1.2 copy-done.6
  137.3 1.2 copy-done.8
  138.6 1.2 copy-done.10
  139.8 1.0 copy-done.13
  140.8 1.0 copy-done.15
  141.9 5.0 %gate_up.1 = bf16[4,256,512]{2,1,0:T(8,128)(2,1)} custom-call(bf16[16,272,256]{2,1,0:T(8,128)(2,1)S(1)} %all-to-all-done.1.refs_0_, bf16[128,4096]{1,0:T(8,128)(2,1)S(1)} %bitcast.23, bf16[128,4096]{1,0:T(8,128)(2,1)S(1)} %copy-done.4, bf16[128,4096]{1,0:T(8,128)(2,1)S(1)} %copy-done.6, bf16[64,4096]{1,0:T(8,128)(2,1)} %collective-permute-done.2.refs_4_, ...), custom_call_target="tpu_custom_call" | custom-call | tf_op jit(solution)/shard_map/gate_up/pallas_call | solution.py:255
  146.8 4.7 %all-to-all-start.2 = ((bf16[4,256,512]{2,1,0:T(8,128)(2,1)}), bf16[4,256,512]{2,1,0:T(8,128)(2,1)S(1)}, u32[]{:S(2)}, u32[]{:S(2)}) async-start(bf16[4,256,512]{2,1,0:T(8,128)(2,1)} %gate_up.1), calls=%async_computation.2 | async-start | bytes 2097152 | tf_op jit(solution)/shard_map/all_to_all | solution.py:272
  152.3 16.5 %all-to-all-done.2.hidden_ref = bf16[4,256,512]{2,1,0:T(8,128)(2,1)S(1)} async-done(((bf16[4,256,512]{2,1,0:T(8,128)(2,1)}), bf16[4,256,512]{2,1,0:T(8,128)(2,1)S(1)}, u32[]{:S(2)}, u32[]{:S(2)}) %all-to-all-start.2) | async-done | bytes 1048608 | tf_op jit(solution)/shard_map/all_to_all | solution.py:272
  168.8 3.4 %down.1 = (bf16[256,256]{1,0:T(8,128)(2,1)S(1)}, bf16[256,256]{1,0:T(8,128)(2,1)S(1)}, bf16[256,256]{1,0:T(8,128)(2,1)S(1)}, bf16[256,256]{1,0:T(8,128)(2,1)S(1)}) custom-call(s32[16]{0:T(128)S(1)} %dynamic-slice_bitcast_fusion.1.idx_ref, bf16[4,256,512]{2,1,0:T(8,128)(2,1)S(1)} %all-to-all-done.2.hidden_ref, bf16[2048,256]{1,0:T(8,128)(2,1)S(1)} %bitcast.32, ...), custom_call_target="tpu_custom_call" | custom-call | tf_op jit(solution)/shard_map/down/pallas_call | solution.py:304
  172.3 2.7 %collective-permute-start.11 = (bf16[256,256]{1,0:T(8,128)(2,1)S(1)}, bf16[256,256]{1,0:T(8,128)(2,1)S(1)}, u32[]{:S(2)}, u32[]{:S(2)}) collective-permute-start(bf16[256,256]{1,0:T(8,128)(2,1)S(1)} %get-tuple-element.16), channel_id=1, source_target_pairs={{0,96},{1,385},{2,98},{3,387},{4,100},{5,389},{6,102},{7,391},{8,1... | collective-permute-start | bytes 393224 | tf_op jit(solution)/shard_map/ppermute | solution.py:39
  175.0 2.6 %collective-permute-start.12 = (bf16[256,256]{1,0:T(8,128)(2,1)S(1)}, bf16[256,256]{1,0:T(8,128)(2,1)S(1)}, u32[]{:S(2)}, u32[]{:S(2)}) collective-permute-start(bf16[256,256]{1,0:T(8,128)(2,1)S(1)} %get-tuple-element.17), channel_id=1, source_target_pairs={{0,32},{1,129},{2,34},{3,131},{4,36},{5,133},{6,38},{7,135},{8,40}... | collective-permute-start | bytes 393224 | tf_op jit(solution)/shard_map/ppermute | solution.py:39
  177.6 1.9 collective-permute-start.13
  179.5 2.4 %collective-permute-done.12.refs_2_ = bf16[256,256]{1,0:T(8,128)(2,1)S(1)} collective-permute-done((bf16[256,256]{1,0:T(8,128)(2,1)S(1)}, bf16[256,256]{1,0:T(8,128)(2,1)S(1)}, u32[]{:S(2)}, u32[]{:S(2)}) %collective-permute-start.12) | collective-permute-done | bytes 131104 | tf_op jit(solution)/shard_map/ppermute | solution.py:39
  181.9 1.5 collective-permute-done.13.refs_3_
  183.5 1.4 gather.1
  184.8 4.9 %all-to-all-start.3 = ((bf16[32,32,256]{2,1,0:T(8,128)(2,1)}), bf16[32,32,256]{2,1,0:T(8,128)(2,1)S(1)}, u32[]{:S(2)}, u32[]{:S(2)}) async-start(bf16[32,32,256]{2,1,0:T(8,128)(2,1)} %bitcast.13), calls=%async_computation.3 | async-start | bytes 1048576 | tf_op jit(solution)/shard_map/all_to_all | solution.py:329
  190.3 33.0 %all-to-all-done.3 = bf16[32,32,256]{2,1,0:T(8,128)(2,1)S(1)} async-done(((bf16[32,32,256]{2,1,0:T(8,128)(2,1)}), bf16[32,32,256]{2,1,0:T(8,128)(2,1)S(1)}, u32[]{:S(2)}, u32[]{:S(2)}) %all-to-all-start.3) | async-done | bytes 524320 | tf_op jit(solution)/shard_map/all_to_all | solution.py:329
  223.3 1.2 combine.1
  224.5 6.2 %all-to-all-start.4 = ((f32[16,1,256]{2,1,0:T(1,128)}), f32[16,1,256]{2,1,0:T(1,128)S(1)}, u32[]{:S(2)}, u32[]{:S(2)}) async-start(f32[16,1,256]{2,1,0:T(1,128)} %get-tuple-element.20), calls=%async_computation.4 | async-start | bytes 32768 | tf_op jit(solution)/shard_map/all_to_all | solution.py:347
  230.7 6.4 %all-to-all-done.4 = f32[16,1,256]{2,1,0:T(1,128)S(1)} async-done(((f32[16,1,256]{2,1,0:T(1,128)}), f32[16,1,256]{2,1,0:T(1,128)S(1)}, u32[]{:S(2)}, u32[]{:S(2)}) %all-to-all-start.4) | async-done | bytes 16416 | tf_op jit(solution)/shard_map/all_to_all | solution.py:347
  (51 shorter events, 2.8 us)
Async XLA Ops:
  0.0 26.4 %copy-start.20 = (s32[2,16]{1,0:T(2,128)S(1)}, s32[2,16]{1,0:T(2,128)}, u32[]{:S(2)}) copy-start(s32[2,16]{1,0:T(2,128)} %constant.89.clone) | copy-start | bytes 388
  0.0 19.0 %copy-start.1 = (bf16[1,128,4096]{2,1,0:T(8,128)(2,1)S(1)}, bf16[1,128,4096]{2,1,0:T(8,128)(2,1)}, u32[]{:S(2)}) copy-start(bf16[1,128,4096]{2,1,0:T(8,128)(2,1)} %param.15) | copy-start | bytes 3145732
  0.0 26.4 %copy-start.18 = (bf16[256]{0:T(256)(128)(2,1)S(1)}, bf16[256]{0:T(256)(128)(2,1)}, u32[]{:S(2)}) copy-start(bf16[256]{0:T(256)(128)(2,1)} %param.12) | copy-start | bytes 1540
  2.3 50.3 %all-to-all-start = ((bf16[32,32,256]{2,1,0:T(8,128)(2,1)}), bf16[32,32,256]{2,1,0:T(8,128)(2,1)S(1)}, u32[]{:S(2)}, u32[]{:S(2)}) async-start(bf16[32,32,256]{2,1,0:T(8,128)(2,1)} %bitcast.4), calls=%async_computation | async-start | bytes 1048576 | tf_op jit(solution)/shard_map/all_to_all | solution.py:219
  20.1 53.6 %collective-permute-start.2 = (bf16[64,4096]{1,0:T(8,128)(2,1)}, bf16[64,4096]{1,0:T(8,128)(2,1)}, u32[]{:S(2)}, u32[]{:S(2)}) collective-permute-start(bf16[64,4096]{1,0:T(8,128)(2,1)} %get-tuple-element.24), channel_id=1, source_target_pairs={{0,384},{1,97},{2,386},{3,99},{4,388},{5,101},{6,390},{7,103},{8,3... | collective-permute-start | bytes 1572872 | tf_op jit(solution)/shard_map/ppermute | solution.py:39
  24.5 51.1 %collective-permute-start.3 = (bf16[64,4096]{1,0:T(8,128)(2,1)}, bf16[64,4096]{1,0:T(8,128)(2,1)}, u32[]{:S(2)}, u32[]{:S(2)}) collective-permute-start(bf16[64,4096]{1,0:T(8,128)(2,1)} %get-tuple-element.23), channel_id=1, source_target_pairs={{0,128},{1,33},{2,130},{3,35},{4,132},{5,37},{6,134},{7,39},{8,136... | collective-permute-start | bytes 1572872 | tf_op jit(solution)/shard_map/ppermute | solution.py:39
  53.2 1.4 copy-start
  54.6 79.1 %all-to-all-start.1 = ((bf16[16,272,256]{2,1,0:T(8,128)(2,1)}), bf16[16,272,256]{2,1,0:T(8,128)(2,1)S(1)}, u32[]{:S(2)}, u32[]{:S(2)}) async-start(bf16[16,272,256]{2,1,0:T(8,128)(2,1)} %copy-done), calls=%async_computation.1 | async-start | bytes 4456448 | tf_op jit(solution)/shard_map/all_to_all | solution.py:253
  62.6 41.2 %collective-permute-start.6 = (bf16[64,4096]{1,0:T(8,128)(2,1)S(1)}, bf16[64,4096]{1,0:T(8,128)(2,1)S(1)}, u32[]{:S(2)}, u32[]{:S(2)}) collective-permute-start(bf16[64,4096]{1,0:T(8,128)(2,1)S(1)} %get-tuple-element.22), channel_id=1, source_target_pairs={{0,384},{1,97},{2,386},{3,99},{4,388},{5,101},{6,390},{7,103},{8,3... | collective-permute-start | bytes 1572872 | tf_op jit(solution)/shard_map/ppermute | solution.py:39
  67.1 56.0 %collective-permute-start = (bf16[128,4096]{1,0:T(8,128)(2,1)S(1)}, bf16[128,4096]{1,0:T(8,128)(2,1)S(1)}, u32[]{:S(2)}, u32[]{:S(2)}) collective-permute-start(bf16[128,4096]{1,0:T(8,128)(2,1)S(1)} %bitcast.21), channel_id=1, source_target_pairs={{0,32},{1,129},{2,34},{3,131},{4,36},{5,133},{6,38},{7,135},{8,40}... | collective-permute-start | bytes 3145736 | tf_op jit(solution)/shard_map/ppermute | solution.py:39
  70.2 56.0 %collective-permute-start.1 = (bf16[128,4096]{1,0:T(8,128)(2,1)S(1)}, bf16[128,4096]{1,0:T(8,128)(2,1)S(1)}, u32[]{:S(2)}, u32[]{:S(2)}) collective-permute-start(bf16[128,4096]{1,0:T(8,128)(2,1)S(1)} %bitcast.22), channel_id=1, source_target_pairs={{0,96},{1,385},{2,98},{3,387},{4,100},{5,389},{6,102},{7,391},{8,1... | collective-permute-start | bytes 3145736 | tf_op jit(solution)/shard_map/ppermute | solution.py:39
  73.7 58.0 %collective-permute-start.4 = (bf16[128,4096]{1,0:T(8,128)(2,1)}, bf16[128,4096]{1,0:T(8,128)(2,1)S(1)}, u32[]{:S(2)}, u32[]{:S(2)}) collective-permute-start(bf16[128,4096]{1,0:T(8,128)(2,1)} %bitcast.24), channel_id=1, source_target_pairs={{0,32},{1,129},{2,34},{3,131},{4,36},{5,133},{6,38},{7,135},{8,40}... | collective-permute-start | bytes 3145736 | tf_op jit(solution)/shard_map/ppermute | solution.py:39
  75.6 57.1 %collective-permute-start.5 = (bf16[128,4096]{1,0:T(8,128)(2,1)}, bf16[128,4096]{1,0:T(8,128)(2,1)S(1)}, u32[]{:S(2)}, u32[]{:S(2)}) collective-permute-start(bf16[128,4096]{1,0:T(8,128)(2,1)} %bitcast.25), channel_id=1, source_target_pairs={{0,96},{1,385},{2,98},{3,387},{4,100},{5,389},{6,102},{7,391},{8,1... | collective-permute-start | bytes 3145736 | tf_op jit(solution)/shard_map/ppermute | solution.py:39
  103.8 0.8 copy-start.12
  104.6 15.4 %collective-permute-start.7 = (bf16[64,4096]{1,0:T(8,128)(2,1)S(1)}, bf16[64,4096]{1,0:T(8,128)(2,1)S(1)}, u32[]{:S(2)}, u32[]{:S(2)}) collective-permute-start(bf16[64,4096]{1,0:T(8,128)(2,1)S(1)} %get-tuple-element.21), channel_id=1, source_target_pairs={{0,128},{1,33},{2,130},{3,35},{4,132},{5,37},{6,134},{7,39},{8,136... | collective-permute-start | bytes 1572872 | tf_op jit(solution)/shard_map/ppermute | solution.py:39
  120.0 0.8 copy-start.14
  120.8 31.4 %collective-permute-start.10 = (bf16[2048,256]{1,0:T(8,128)(2,1)}, bf16[2048,256]{1,0:T(8,128)(2,1)}, u32[]{:S(2)}, u32[]{:S(2)}) collective-permute-start(bf16[2048,256]{1,0:T(8,128)(2,1)} %bitcast.29), channel_id=1, source_target_pairs={{0,128},{1,33},{2,130},{3,35},{4,132},{5,37},{6,134},{7,39},{8,136... | collective-permute-start | bytes 3145736 | tf_op jit(solution)/shard_map/ppermute | solution.py:39
  123.2 1.0 copy-start.3
  124.2 28.1 %collective-permute-start.8 = (bf16[2048,256]{1,0:T(8,128)(2,1)}, bf16[2048,256]{1,0:T(8,128)(2,1)}, u32[]{:S(2)}, u32[]{:S(2)}) collective-permute-start(bf16[2048,256]{1,0:T(8,128)(2,1)} %bitcast.30), channel_id=1, source_target_pairs={{0,32},{1,129},{2,34},{3,131},{4,36},{5,133},{6,38},{7,135},{8,40}... | collective-permute-start | bytes 3145736 | tf_op jit(solution)/shard_map/ppermute | solution.py:39
  126.2 1.0 copy-start.5
  127.2 25.1 %collective-permute-start.9 = (bf16[2048,256]{1,0:T(8,128)(2,1)}, bf16[2048,256]{1,0:T(8,128)(2,1)}, u32[]{:S(2)}, u32[]{:S(2)}) collective-permute-start(bf16[2048,256]{1,0:T(8,128)(2,1)} %bitcast.31), channel_id=1, source_target_pairs={{0,96},{1,385},{2,98},{3,387},{4,100},{5,389},{6,102},{7,391},{8,1... | collective-permute-start | bytes 3145736 | tf_op jit(solution)/shard_map/ppermute | solution.py:39
  131.7 1.1 copy-start.7
  132.7 1.0 copy-start.9
  133.7 1.2 copy-start.2
  134.9 1.2 copy-start.4
  136.1 1.2 copy-start.6
  137.3 1.2 copy-start.8
  138.6 1.2 copy-start.10
  139.8 1.0 copy-start.13
  140.8 1.0 copy-start.15
  146.8 22.0 %copy-start.11 = (bf16[1,2048,256]{2,1,0:T(8,128)(2,1)S(1)}, bf16[1,2048,256]{2,1,0:T(8,128)(2,1)}, u32[]{:S(2)}) copy-start(bf16[1,2048,256]{2,1,0:T(8,128)(2,1)} %param.17) | copy-start | bytes 3145732
  146.8 22.0 %all-to-all-start.2 = ((bf16[4,256,512]{2,1,0:T(8,128)(2,1)}), bf16[4,256,512]{2,1,0:T(8,128)(2,1)S(1)}, u32[]{:S(2)}, u32[]{:S(2)}) async-start(bf16[4,256,512]{2,1,0:T(8,128)(2,1)} %gate_up.1), calls=%async_computation.2 | async-start | bytes 2097152 | tf_op jit(solution)/shard_map/all_to_all | solution.py:272
  152.3 27.2 %copy-start.21 = (s32[4]{0:T(128)S(1)}, s32[4]{0:T(128)}, u32[]{:S(2)}) copy-start(s32[4]{0:T(128)} %constant.91.clone) | copy-start | bytes 52
  152.3 37.5 %copy-start.16 = (s32[256,2]{0,1:T(2,128)S(1)}, s32[256,2]{0,1:T(2,128)}, u32[]{:S(2)}) copy-start(s32[256,2]{0,1:T(2,128)} %param.13) | copy-start | bytes 6148
  152.3 37.5 %copy-start.17 = (f32[256,2]{0,1:T(2,128)S(1)}, f32[256,2]{0,1:T(2,128)}, u32[]{:S(2)}) copy-start(f32[256,2]{0,1:T(2,128)} %param.14) | copy-start | bytes 6148
  172.3 58.5 %copy-start.19 = (bf16[256]{0:T(256)(128)(2,1)S(1)}, bf16[256]{0:T(256)(128)(2,1)}, u32[]{:S(2)}) copy-start(bf16[256]{0:T(256)(128)(2,1)} %param.18) | copy-start | bytes 1540
  172.3 7.3 %collective-permute-start.11 = (bf16[256,256]{1,0:T(8,128)(2,1)S(1)}, bf16[256,256]{1,0:T(8,128)(2,1)S(1)}, u32[]{:S(2)}, u32[]{:S(2)}) collective-permute-start(bf16[256,256]{1,0:T(8,128)(2,1)S(1)} %get-tuple-element.16), channel_id=1, source_target_pairs={{0,96},{1,385},{2,98},{3,387},{4,100},{5,389},{6,102},{7,391},{8,1... | collective-permute-start | bytes 393224 | tf_op jit(solution)/shard_map/ppermute | solution.py:39
  175.0 6.9 %collective-permute-start.12 = (bf16[256,256]{1,0:T(8,128)(2,1)S(1)}, bf16[256,256]{1,0:T(8,128)(2,1)S(1)}, u32[]{:S(2)}, u32[]{:S(2)}) collective-permute-start(bf16[256,256]{1,0:T(8,128)(2,1)S(1)} %get-tuple-element.17), channel_id=1, source_target_pairs={{0,32},{1,129},{2,34},{3,131},{4,36},{5,133},{6,38},{7,135},{8,40}... | collective-permute-start | bytes 393224 | tf_op jit(solution)/shard_map/ppermute | solution.py:39
  177.6 5.9 %collective-permute-start.13 = (bf16[256,256]{1,0:T(8,128)(2,1)S(1)}, bf16[256,256]{1,0:T(8,128)(2,1)S(1)}, u32[]{:S(2)}, u32[]{:S(2)}) collective-permute-start(bf16[256,256]{1,0:T(8,128)(2,1)S(1)} %get-tuple-element.18), channel_id=1, source_target_pairs={{0,384},{1,97},{2,386},{3,99},{4,388},{5,101},{6,390},{7,103},{8,3... | collective-permute-start | bytes 393224 | tf_op jit(solution)/shard_map/ppermute | solution.py:39
  184.8 38.5 %all-to-all-start.3 = ((bf16[32,32,256]{2,1,0:T(8,128)(2,1)}), bf16[32,32,256]{2,1,0:T(8,128)(2,1)S(1)}, u32[]{:S(2)}, u32[]{:S(2)}) async-start(bf16[32,32,256]{2,1,0:T(8,128)(2,1)} %bitcast.13), calls=%async_computation.3 | async-start | bytes 1048576 | tf_op jit(solution)/shard_map/all_to_all | solution.py:329
  224.5 12.7 %all-to-all-start.4 = ((f32[16,1,256]{2,1,0:T(1,128)}), f32[16,1,256]{2,1,0:T(1,128)S(1)}, u32[]{:S(2)}, u32[]{:S(2)}) async-start(f32[16,1,256]{2,1,0:T(1,128)} %get-tuple-element.20), calls=%async_computation.4 | async-start | bytes 32768 | tf_op jit(solution)/shard_map/all_to_all | solution.py:347

commit v3 on v2

--- a/solution.py
+++ b/solution.py
@@ -148,9 +148,9 @@
 
 
 def down_kernel(idx_ref, hidden_ref, *refs, pieces):
-    weights = refs[:pieces]
-    outs = refs[pieces : 2 * pieces]
-    ordered = refs[2 * pieces]
+    weights = refs[: pieces - 1]
+    outs = refs[pieces - 1 : 2 * pieces - 2]
+    ordered = refs[2 * pieces - 2]
     units = hidden_ref.shape[2] // pieces
     for p in range(hidden_ref.shape[0]):
         for n in range(pieces):
@@ -163,10 +163,16 @@
                     lane < units // 2, part.astype(jnp.float32), other.astype(jnp.float32)
                 ).astype(jnp.bfloat16)
             ordered[:, pl.ds(at, units)] = part
-    for n in range(pieces):
+    for n in range(pieces - 1):
         outs[n][...] = jnp.dot(
             ordered[...], weights[n][...], preferred_element_type=jnp.float32
         ).astype(jnp.bfloat16)
+
+
+def own_kernel(ordered_ref, weight_ref, out_ref):
+    out_ref[...] = jnp.dot(
+        ordered_ref[...], weight_ref[...], preferred_element_type=jnp.float32
+    ).astype(jnp.bfloat16)
 
 
 def gather_kernel(q_ref, *refs):
@@ -301,20 +307,27 @@
     ).reshape(2 * CLASSES, SIDE * pieces)
     order = lax.dynamic_index_in_dim(table, core * CLASSES + mine, 0, keepdims=False)
 
-    outs = pl.pallas_call(
+    *outs, ordered = pl.pallas_call(
         functools.partial(down_kernel, pieces=pieces),
-        out_shape=[pltpu.VMEM((rows, local), jnp.bfloat16)] * pieces,
-        in_specs=[smem] + [vmem] * (1 + pieces),
+        out_shape=[
+            *[pltpu.VMEM((rows, local), jnp.bfloat16)] * (pieces - 1),
+            pltpu.VMEM((rows, hidden_all), jnp.bfloat16),
+        ],
+        in_specs=[smem] + [vmem] * pieces,
         out_specs=[vmem] * pieces,
-        scratch_shapes=[pltpu.VMEM((rows, hidden_all), jnp.bfloat16)],
         compiler_params=pltpu.CompilerParams(vmem_limit_bytes=GRANT),
         name="down",
-    )(order, in_vmem(shared), *(in_vmem(w) for w in downs))
-
-    pieces_back = [
-        outs[0],
-        *(shifted(out, -dy, -dx) for out, (dy, dx) in zip(outs[1:], last_steps)),
-    ]
+    )(order, in_vmem(shared), *(in_vmem(w) for w in downs[1:]))
+    backs = [shifted(out, -dy, -dx) for out, (dy, dx) in zip(outs, last_steps)]
+    own = pl.pallas_call(
+        own_kernel,
+        out_shape=pltpu.VMEM((rows, local), jnp.bfloat16),
+        in_specs=[vmem] * 2,
+        out_specs=vmem,
+        compiler_params=pltpu.CompilerParams(vmem_limit_bytes=GRANT),
+        name="own",
+    )(in_vmem(ordered), in_vmem(downs[0]))
+    pieces_back = [own, *backs]
     places = jnp.asarray([0, *(dx + 2 * dy for dy, dx in last_steps)], jnp.int32)
     places = (mine + places) % CLASSES
     returned = pl.pallas_call(

time: 239 us -> 239 us (level)
  no operation moved by 1% of the time
where the time goes in v3:
time: 239 us; the launch traced here: 238 us
  waiting for transfers between devices  123 us (51%)
  starting transfers between devices  80.9 us (34%)
  local copies, waits for them, and re-layouts  18.3 us (8%)
  Pallas kernels  14.6 us (6%)
    ppermute x14, starting transfers between devices, shifted(): return lax.ppermute(value, ('ep', 'tp'), pairs)  41.7 us
    ppermute x14, waiting for transfers between devices, shifted(): return lax.ppermute(value, ('ep', 'tp'), pairs)  40.6 us
    all_to_all x1, waiting for transfers between devices, body(): lax.all_to_all(returned.reshape(n_route, capacity, local), 'tp', split_ax...  33 us
    all_to_all x1, waiting for transfers between devices, body(): lax.all_to_all(buffer.reshape(experts, capacity, local), 'tp', split_axis...  26.1 us
    all_to_all x1, starting transfers between devices, body(): lax.all_to_all(buffer.reshape(experts, capacity, local), 'tp', split_axis...  16.7 us
    all_to_all x1, waiting for transfers between devices, body(): lax.all_to_all(hidden, ('ep', 'tp'), split_axis=0, concat_axis=0, tiled=T...  16.5 us
    unnamed x44, local copies, waits for them, and re-layouts  15.1 us
    all_to_all x1, starting transfers between devices, body(): lax.all_to_all(operand, 'ep', split_axis=0, concat_axis=0, tiled=True)  6.75 us
  transfers between devices with their start and end apart: 19, of which 8 were waited for; matrix products, arithmetic and copies ran while one was open for 1% of the time, Pallas kernels for 3%

profile of v3, /device:TPU:1, one launch (start us, length us, event | category | flops | bytes accessed | tf_op | source)
XLA Modules:
  0.0 237.6 jit_solution(9865709840558765058)
XLA Ops:
  0.0 2.3 dispatch.1
  2.3 16.7 %all-to-all-start = ((bf16[32,32,256]{2,1,0:T(8,128)(2,1)}), bf16[32,32,256]{2,1,0:T(8,128)(2,1)S(1)}, u32[]{:S(2)}, u32[]{:S(2)}) async-start(bf16[32,32,256]{2,1,0:T(8,128)(2,1)} %bitcast.4), calls=%async_computation | async-start | bytes 1048576 | tf_op jit(solution)/shard_map/all_to_all | solution.py:225
  19.0 1.1 slice_bitcast_fusion.2
  20.1 4.4 %collective-permute-start.2 = (bf16[64,4096]{1,0:T(8,128)(2,1)}, bf16[64,4096]{1,0:T(8,128)(2,1)}, u32[]{:S(2)}, u32[]{:S(2)}) collective-permute-start(bf16[64,4096]{1,0:T(8,128)(2,1)} %get-tuple-element.24), channel_id=1, source_target_pairs={{0,384},{1,97},{2,386},{3,99},{4,388},{5,101},{6,390},{7,103},{8,3... | collective-permute-start | bytes 1572872 | tf_op jit(solution)/shard_map/ppermute | solution.py:39
  24.5 1.9 collective-permute-start.3
  26.5 26.1 %all-to-all-done = bf16[32,32,256]{2,1,0:T(8,128)(2,1)S(1)} async-done(((bf16[32,32,256]{2,1,0:T(8,128)(2,1)}), bf16[32,32,256]{2,1,0:T(8,128)(2,1)S(1)}, u32[]{:S(2)}, u32[]{:S(2)}) %all-to-all-start) | async-done | bytes 524320 | tf_op jit(solution)/shard_map/all_to_all | solution.py:225
  53.2 1.4 copy-done
  54.6 6.7 %all-to-all-start.1 = ((bf16[16,272,256]{2,1,0:T(8,128)(2,1)}), bf16[16,272,256]{2,1,0:T(8,128)(2,1)S(1)}, u32[]{:S(2)}, u32[]{:S(2)}) async-start(bf16[16,272,256]{2,1,0:T(8,128)(2,1)} %copy-done), calls=%async_computation.1 | async-start | bytes 4456448 | tf_op jit(solution)/shard_map/all_to_all | solution.py:259
  61.4 1.3 slice_bitcast_fusion
  62.6 4.5 %collective-permute-start.6 = (bf16[64,4096]{1,0:T(8,128)(2,1)S(1)}, bf16[64,4096]{1,0:T(8,128)(2,1)S(1)}, u32[]{:S(2)}, u32[]{:S(2)}) collective-permute-start(bf16[64,4096]{1,0:T(8,128)(2,1)S(1)} %get-tuple-element.22), channel_id=1, source_target_pairs={{0,384},{1,97},{2,386},{3,99},{4,388},{5,101},{6,390},{7,103},{8,3... | collective-permute-start | bytes 1572872 | tf_op jit(solution)/shard_map/ppermute | solution.py:39
  67.1 3.1 %collective-permute-start = (bf16[128,4096]{1,0:T(8,128)(2,1)S(1)}, bf16[128,4096]{1,0:T(8,128)(2,1)S(1)}, u32[]{:S(2)}, u32[]{:S(2)}) collective-permute-start(bf16[128,4096]{1,0:T(8,128)(2,1)S(1)} %bitcast.21), channel_id=1, source_target_pairs={{0,32},{1,129},{2,34},{3,131},{4,36},{5,133},{6,38},{7,135},{8,40}... | collective-permute-start | bytes 3145736 | tf_op jit(solution)/shard_map/ppermute | solution.py:39
  70.2 3.4 %collective-permute-start.1 = (bf16[128,4096]{1,0:T(8,128)(2,1)S(1)}, bf16[128,4096]{1,0:T(8,128)(2,1)S(1)}, u32[]{:S(2)}, u32[]{:S(2)}) collective-permute-start(bf16[128,4096]{1,0:T(8,128)(2,1)S(1)} %bitcast.22), channel_id=1, source_target_pairs={{0,96},{1,385},{2,98},{3,387},{4,100},{5,389},{6,102},{7,391},{8,1... | collective-permute-start | bytes 3145736 | tf_op jit(solution)/shard_map/ppermute | solution.py:39
  73.7 1.9 collective-permute-start.4
  75.6 4.6 %collective-permute-start.5 = (bf16[128,4096]{1,0:T(8,128)(2,1)}, bf16[128,4096]{1,0:T(8,128)(2,1)S(1)}, u32[]{:S(2)}, u32[]{:S(2)}) collective-permute-start(bf16[128,4096]{1,0:T(8,128)(2,1)} %bitcast.25), channel_id=1, source_target_pairs={{0,96},{1,385},{2,98},{3,387},{4,100},{5,389},{6,102},{7,391},{8,1... | collective-permute-start | bytes 3145736 | tf_op jit(solution)/shard_map/ppermute | solution.py:39
  80.2 23.7 %collective-permute-done.6.refs_9_ = bf16[64,4096]{1,0:T(8,128)(2,1)S(1)} collective-permute-done((bf16[64,4096]{1,0:T(8,128)(2,1)S(1)}, bf16[64,4096]{1,0:T(8,128)(2,1)S(1)}, u32[]{:S(2)}, u32[]{:S(2)}) %collective-permute-start.6) | collective-permute-done | bytes 524320 | tf_op jit(solution)/shard_map/ppermute | solution.py:39
  103.8 0.8 copy-done.12
  104.6 1.9 collective-permute-start.7
  106.6 13.5 %collective-permute-done.7.refs_10_ = bf16[64,4096]{1,0:T(8,128)(2,1)S(1)} collective-permute-done((bf16[64,4096]{1,0:T(8,128)(2,1)S(1)}, bf16[64,4096]{1,0:T(8,128)(2,1)S(1)}, u32[]{:S(2)}, u32[]{:S(2)}) %collective-permute-start.7) | collective-permute-done | bytes 524320 | tf_op jit(solution)/shard_map/ppermute | solution.py:39
  120.0 0.8 copy-done.14
  120.8 2.3 collective-permute-start.10
  123.2 1.0 copy-done.3
  124.2 2.0 collective-permute-start.8
  126.2 1.0 copy-done.5
  127.2 4.4 %collective-permute-start.9 = (bf16[2048,256]{1,0:T(8,128)(2,1)}, bf16[2048,256]{1,0:T(8,128)(2,1)}, u32[]{:S(2)}, u32[]{:S(2)}) collective-permute-start(bf16[2048,256]{1,0:T(8,128)(2,1)} %bitcast.31), channel_id=1, source_target_pairs={{0,96},{1,385},{2,98},{3,387},{4,100},{5,389},{6,102},{7,391},{8,1... | collective-permute-start | bytes 3145736 | tf_op jit(solution)/shard_map/ppermute | solution.py:39
  131.7 1.0 copy-done.7
  132.7 1.0 copy-done.9
  133.7 1.2 copy-done.2
  134.9 1.2 copy-done.4
  136.1 1.2 copy-done.6
  137.3 1.2 copy-done.8
  138.6 1.2 copy-done.10
  139.8 1.0 copy-done.13
  140.8 1.0 copy-done.15
  141.9 5.0 %gate_up.1 = bf16[4,256,512]{2,1,0:T(8,128)(2,1)} custom-call(bf16[16,272,256]{2,1,0:T(8,128)(2,1)S(1)} %all-to-all-done.1.refs_0_, bf16[128,4096]{1,0:T(8,128)(2,1)S(1)} %bitcast.23, bf16[128,4096]{1,0:T(8,128)(2,1)S(1)} %copy-done.4, bf16[128,4096]{1,0:T(8,128)(2,1)S(1)} %copy-done.6, bf16[64,4096]{1,0:T(8,128)(2,1)} %collective-permute-done.2.refs_4_, ...), custom_call_target="tpu_custom_call" | custom-call | tf_op jit(solution)/shard_map/gate_up/pallas_call | solution.py:261
  146.8 4.6 %all-to-all-start.2 = ((bf16[4,256,512]{2,1,0:T(8,128)(2,1)}), bf16[4,256,512]{2,1,0:T(8,128)(2,1)S(1)}, u32[]{:S(2)}, u32[]{:S(2)}) async-start(bf16[4,256,512]{2,1,0:T(8,128)(2,1)} %gate_up.1), calls=%async_computation.2 | async-start | bytes 2097152 | tf_op jit(solution)/shard_map/all_to_all | solution.py:278
  152.2 16.5 %all-to-all-done.2.hidden_ref = bf16[4,256,512]{2,1,0:T(8,128)(2,1)S(1)} async-done(((bf16[4,256,512]{2,1,0:T(8,128)(2,1)}), bf16[4,256,512]{2,1,0:T(8,128)(2,1)S(1)}, u32[]{:S(2)}, u32[]{:S(2)}) %all-to-all-start.2) | async-done | bytes 1048608 | tf_op jit(solution)/shard_map/all_to_all | solution.py:278
  168.7 3.2 %down.1 = (bf16[256,256]{1,0:T(8,128)(2,1)S(1)}, bf16[256,256]{1,0:T(8,128)(2,1)S(1)}, bf16[256,256]{1,0:T(8,128)(2,1)S(1)}, bf16[256,2048]{1,0:T(8,128)(2,1)S(1)}) custom-call(s32[16]{0:T(128)S(1)} %dynamic-slice_bitcast_fusion.1.idx_ref, bf16[4,256,512]{2,1,0:T(8,128)(2,1)S(1)} %all-to-all-done.2.hidden_ref, ...), custom_call_target="tpu_custom_call" | custom-call | tf_op jit(solution)/shard_map/down/pallas_call | solution.py:310
  171.9 2.7 %collective-permute-start.11 = (bf16[256,256]{1,0:T(8,128)(2,1)S(1)}, bf16[256,256]{1,0:T(8,128)(2,1)S(1)}, u32[]{:S(2)}, u32[]{:S(2)}) collective-permute-start(bf16[256,256]{1,0:T(8,128)(2,1)S(1)} %get-tuple-element.16), channel_id=1, source_target_pairs={{0,96},{1,385},{2,98},{3,387},{4,100},{5,389},{6,102},{7,391},{8,1... | collective-permute-start | bytes 393224 | tf_op jit(solution)/shard_map/ppermute | solution.py:39
  174.6 2.6 %collective-permute-start.12 = (bf16[256,256]{1,0:T(8,128)(2,1)S(1)}, bf16[256,256]{1,0:T(8,128)(2,1)S(1)}, u32[]{:S(2)}, u32[]{:S(2)}) collective-permute-start(bf16[256,256]{1,0:T(8,128)(2,1)S(1)} %get-tuple-element.17), channel_id=1, source_target_pairs={{0,32},{1,129},{2,34},{3,131},{4,36},{5,133},{6,38},{7,135},{8,40}... | collective-permute-start | bytes 393224 | tf_op jit(solution)/shard_map/ppermute | solution.py:39
  177.2 1.9 collective-permute-start.13
  179.6 1.9 collective-permute-done.12.refs_2_
  181.5 1.5 collective-permute-done.13.refs_3_
  183.1 1.4 gather.1
  184.4 4.9 %all-to-all-start.3 = ((bf16[32,32,256]{2,1,0:T(8,128)(2,1)}), bf16[32,32,256]{2,1,0:T(8,128)(2,1)S(1)}, u32[]{:S(2)}, u32[]{:S(2)}) async-start(bf16[32,32,256]{2,1,0:T(8,128)(2,1)} %bitcast.13), calls=%async_computation.3 | async-start | bytes 1048576 | tf_op jit(solution)/shard_map/all_to_all | solution.py:342
  189.9 33.0 %all-to-all-done.3 = bf16[32,32,256]{2,1,0:T(8,128)(2,1)S(1)} async-done(((bf16[32,32,256]{2,1,0:T(8,128)(2,1)}), bf16[32,32,256]{2,1,0:T(8,128)(2,1)S(1)}, u32[]{:S(2)}, u32[]{:S(2)}) %all-to-all-start.3) | async-done | bytes 524320 | tf_op jit(solution)/shard_map/all_to_all | solution.py:342
  222.9 1.2 combine.1
  224.1 6.2 %all-to-all-start.4 = ((f32[16,1,256]{2,1,0:T(1,128)}), f32[16,1,256]{2,1,0:T(1,128)S(1)}, u32[]{:S(2)}, u32[]{:S(2)}) async-start(f32[16,1,256]{2,1,0:T(1,128)} %get-tuple-element.20), calls=%async_computation.4 | async-start | bytes 32768 | tf_op jit(solution)/shard_map/all_to_all | solution.py:360
  230.3 6.4 %all-to-all-done.4 = f32[16,1,256]{2,1,0:T(1,128)S(1)} async-done(((f32[16,1,256]{2,1,0:T(1,128)}), f32[16,1,256]{2,1,0:T(1,128)S(1)}, u32[]{:S(2)}, u32[]{:S(2)}) %all-to-all-start.4) | async-done | bytes 16416 | tf_op jit(solution)/shard_map/all_to_all | solution.py:360
  (52 shorter events, 3.3 us)
Async XLA Ops:
  0.0 26.4 %copy-start.20 = (s32[2,16]{1,0:T(2,128)S(1)}, s32[2,16]{1,0:T(2,128)}, u32[]{:S(2)}) copy-start(s32[2,16]{1,0:T(2,128)} %constant.89.clone) | copy-start | bytes 388
  0.0 19.0 %copy-start.1 = (bf16[1,128,4096]{2,1,0:T(8,128)(2,1)S(1)}, bf16[1,128,4096]{2,1,0:T(8,128)(2,1)}, u32[]{:S(2)}) copy-start(bf16[1,128,4096]{2,1,0:T(8,128)(2,1)} %param.15) | copy-start | bytes 3145732
  0.0 26.4 %copy-start.18 = (bf16[256]{0:T(256)(128)(2,1)S(1)}, bf16[256]{0:T(256)(128)(2,1)}, u32[]{:S(2)}) copy-start(bf16[256]{0:T(256)(128)(2,1)} %param.12) | copy-start | bytes 1540
  2.3 50.3 %all-to-all-start = ((bf16[32,32,256]{2,1,0:T(8,128)(2,1)}), bf16[32,32,256]{2,1,0:T(8,128)(2,1)S(1)}, u32[]{:S(2)}, u32[]{:S(2)}) async-start(bf16[32,32,256]{2,1,0:T(8,128)(2,1)} %bitcast.4), calls=%async_computation | async-start | bytes 1048576 | tf_op jit(solution)/shard_map/all_to_all | solution.py:225
  20.1 53.6 %collective-permute-start.2 = (bf16[64,4096]{1,0:T(8,128)(2,1)}, bf16[64,4096]{1,0:T(8,128)(2,1)}, u32[]{:S(2)}, u32[]{:S(2)}) collective-permute-start(bf16[64,4096]{1,0:T(8,128)(2,1)} %get-tuple-element.24), channel_id=1, source_target_pairs={{0,384},{1,97},{2,386},{3,99},{4,388},{5,101},{6,390},{7,103},{8,3... | collective-permute-start | bytes 1572872 | tf_op jit(solution)/shard_map/ppermute | solution.py:39
  24.5 51.1 %collective-permute-start.3 = (bf16[64,4096]{1,0:T(8,128)(2,1)}, bf16[64,4096]{1,0:T(8,128)(2,1)}, u32[]{:S(2)}, u32[]{:S(2)}) collective-permute-start(bf16[64,4096]{1,0:T(8,128)(2,1)} %get-tuple-element.23), channel_id=1, source_target_pairs={{0,128},{1,33},{2,130},{3,35},{4,132},{5,37},{6,134},{7,39},{8,136... | collective-permute-start | bytes 1572872 | tf_op jit(solution)/shard_map/ppermute | solution.py:39
  53.2 1.4 copy-start
  54.6 79.1 %all-to-all-start.1 = ((bf16[16,272,256]{2,1,0:T(8,128)(2,1)}), bf16[16,272,256]{2,1,0:T(8,128)(2,1)S(1)}, u32[]{:S(2)}, u32[]{:S(2)}) async-start(bf16[16,272,256]{2,1,0:T(8,128)(2,1)} %copy-done), calls=%async_computation.1 | async-start | bytes 4456448 | tf_op jit(solution)/shard_map/all_to_all | solution.py:259
  62.6 41.2 %collective-permute-start.6 = (bf16[64,4096]{1,0:T(8,128)(2,1)S(1)}, bf16[64,4096]{1,0:T(8,128)(2,1)S(1)}, u32[]{:S(2)}, u32[]{:S(2)}) collective-permute-start(bf16[64,4096]{1,0:T(8,128)(2,1)S(1)} %get-tuple-element.22), channel_id=1, source_target_pairs={{0,384},{1,97},{2,386},{3,99},{4,388},{5,101},{6,390},{7,103},{8,3... | collective-permute-start | bytes 1572872 | tf_op jit(solution)/shard_map/ppermute | solution.py:39
  67.1 56.0 %collective-permute-start = (bf16[128,4096]{1,0:T(8,128)(2,1)S(1)}, bf16[128,4096]{1,0:T(8,128)(2,1)S(1)}, u32[]{:S(2)}, u32[]{:S(2)}) collective-permute-start(bf16[128,4096]{1,0:T(8,128)(2,1)S(1)} %bitcast.21), channel_id=1, source_target_pairs={{0,32},{1,129},{2,34},{3,131},{4,36},{5,133},{6,38},{7,135},{8,40}... | collective-permute-start | bytes 3145736 | tf_op jit(solution)/shard_map/ppermute | solution.py:39
  70.2 56.0 %collective-permute-start.1 = (bf16[128,4096]{1,0:T(8,128)(2,1)S(1)}, bf16[128,4096]{1,0:T(8,128)(2,1)S(1)}, u32[]{:S(2)}, u32[]{:S(2)}) collective-permute-start(bf16[128,4096]{1,0:T(8,128)(2,1)S(1)} %bitcast.22), channel_id=1, source_target_pairs={{0,96},{1,385},{2,98},{3,387},{4,100},{5,389},{6,102},{7,391},{8,1... | collective-permute-start | bytes 3145736 | tf_op jit(solution)/shard_map/ppermute | solution.py:39
  73.7 58.0 %collective-permute-start.4 = (bf16[128,4096]{1,0:T(8,128)(2,1)}, bf16[128,4096]{1,0:T(8,128)(2,1)S(1)}, u32[]{:S(2)}, u32[]{:S(2)}) collective-permute-start(bf16[128,4096]{1,0:T(8,128)(2,1)} %bitcast.24), channel_id=1, source_target_pairs={{0,32},{1,129},{2,34},{3,131},{4,36},{5,133},{6,38},{7,135},{8,40}... | collective-permute-start | bytes 3145736 | tf_op jit(solution)/shard_map/ppermute | solution.py:39
  75.6 57.1 %collective-permute-start.5 = (bf16[128,4096]{1,0:T(8,128)(2,1)}, bf16[128,4096]{1,0:T(8,128)(2,1)S(1)}, u32[]{:S(2)}, u32[]{:S(2)}) collective-permute-start(bf16[128,4096]{1,0:T(8,128)(2,1)} %bitcast.25), channel_id=1, source_target_pairs={{0,96},{1,385},{2,98},{3,387},{4,100},{5,389},{6,102},{7,391},{8,1... | collective-permute-start | bytes 3145736 | tf_op jit(solution)/shard_map/ppermute | solution.py:39
  103.8 0.8 copy-start.12
  104.6 15.4 %collective-permute-start.7 = (bf16[64,4096]{1,0:T(8,128)(2,1)S(1)}, bf16[64,4096]{1,0:T(8,128)(2,1)S(1)}, u32[]{:S(2)}, u32[]{:S(2)}) collective-permute-start(bf16[64,4096]{1,0:T(8,128)(2,1)S(1)} %get-tuple-element.21), channel_id=1, source_target_pairs={{0,128},{1,33},{2,130},{3,35},{4,132},{5,37},{6,134},{7,39},{8,136... | collective-permute-start | bytes 1572872 | tf_op jit(solution)/shard_map/ppermute | solution.py:39
  120.0 0.8 copy-start.14
  120.8 31.4 %collective-permute-start.10 = (bf16[2048,256]{1,0:T(8,128)(2,1)}, bf16[2048,256]{1,0:T(8,128)(2,1)}, u32[]{:S(2)}, u32[]{:S(2)}) collective-permute-start(bf16[2048,256]{1,0:T(8,128)(2,1)} %bitcast.29), channel_id=1, source_target_pairs={{0,128},{1,33},{2,130},{3,35},{4,132},{5,37},{6,134},{7,39},{8,136... | collective-permute-start | bytes 3145736 | tf_op jit(solution)/shard_map/ppermute | solution.py:39
  123.2 1.0 copy-start.3
  124.2 28.1 %collective-permute-start.8 = (bf16[2048,256]{1,0:T(8,128)(2,1)}, bf16[2048,256]{1,0:T(8,128)(2,1)}, u32[]{:S(2)}, u32[]{:S(2)}) collective-permute-start(bf16[2048,256]{1,0:T(8,128)(2,1)} %bitcast.30), channel_id=1, source_target_pairs={{0,32},{1,129},{2,34},{3,131},{4,36},{5,133},{6,38},{7,135},{8,40}... | collective-permute-start | bytes 3145736 | tf_op jit(solution)/shard_map/ppermute | solution.py:39
  126.2 1.0 copy-start.5
  127.2 25.0 %collective-permute-start.9 = (bf16[2048,256]{1,0:T(8,128)(2,1)}, bf16[2048,256]{1,0:T(8,128)(2,1)}, u32[]{:S(2)}, u32[]{:S(2)}) collective-permute-start(bf16[2048,256]{1,0:T(8,128)(2,1)} %bitcast.31), channel_id=1, source_target_pairs={{0,96},{1,385},{2,98},{3,387},{4,100},{5,389},{6,102},{7,391},{8,1... | collective-permute-start | bytes 3145736 | tf_op jit(solution)/shard_map/ppermute | solution.py:39
  131.7 1.1 copy-start.7
  132.7 1.0 copy-start.9
  133.7 1.2 copy-start.2
  134.9 1.2 copy-start.4
  136.1 1.2 copy-start.6
  137.3 1.2 copy-start.8
  138.6 1.2 copy-start.10
  139.8 1.0 copy-start.13
  140.8 1.0 copy-start.15
  146.8 21.8 %all-to-all-start.2 = ((bf16[4,256,512]{2,1,0:T(8,128)(2,1)}), bf16[4,256,512]{2,1,0:T(8,128)(2,1)S(1)}, u32[]{:S(2)}, u32[]{:S(2)}) async-start(bf16[4,256,512]{2,1,0:T(8,128)(2,1)} %gate_up.1), calls=%async_computation.2 | async-start | bytes 2097152 | tf_op jit(solution)/shard_map/all_to_all | solution.py:278
  151.4 27.7 %copy-start.21 = (s32[4]{0:T(128)S(1)}, s32[4]{0:T(128)}, u32[]{:S(2)}) copy-start(s32[4]{0:T(128)} %constant.91.clone) | copy-start | bytes 52
  151.4 27.7 %copy-start.11 = (bf16[1,2048,256]{2,1,0:T(8,128)(2,1)S(1)}, bf16[1,2048,256]{2,1,0:T(8,128)(2,1)}, u32[]{:S(2)}) copy-start(bf16[1,2048,256]{2,1,0:T(8,128)(2,1)} %param.17) | copy-start | bytes 3145732
  171.9 17.5 %copy-start.16 = (s32[256,2]{0,1:T(2,128)S(1)}, s32[256,2]{0,1:T(2,128)}, u32[]{:S(2)}) copy-start(s32[256,2]{0,1:T(2,128)} %param.13) | copy-start | bytes 6148
  171.9 17.5 %copy-start.17 = (f32[256,2]{0,1:T(2,128)S(1)}, f32[256,2]{0,1:T(2,128)}, u32[]{:S(2)}) copy-start(f32[256,2]{0,1:T(2,128)} %param.14) | copy-start | bytes 6148
  171.9 7.7 %collective-permute-start.11 = (bf16[256,256]{1,0:T(8,128)(2,1)S(1)}, bf16[256,256]{1,0:T(8,128)(2,1)S(1)}, u32[]{:S(2)}, u32[]{:S(2)}) collective-permute-start(bf16[256,256]{1,0:T(8,128)(2,1)S(1)} %get-tuple-element.16), channel_id=1, source_target_pairs={{0,96},{1,385},{2,98},{3,387},{4,100},{5,389},{6,102},{7,391},{8,1... | collective-permute-start | bytes 393224 | tf_op jit(solution)/shard_map/ppermute | solution.py:39
  174.6 6.9 %collective-permute-start.12 = (bf16[256,256]{1,0:T(8,128)(2,1)S(1)}, bf16[256,256]{1,0:T(8,128)(2,1)S(1)}, u32[]{:S(2)}, u32[]{:S(2)}) collective-permute-start(bf16[256,256]{1,0:T(8,128)(2,1)S(1)} %get-tuple-element.17), channel_id=1, source_target_pairs={{0,32},{1,129},{2,34},{3,131},{4,36},{5,133},{6,38},{7,135},{8,40}... | collective-permute-start | bytes 393224 | tf_op jit(solution)/shard_map/ppermute | solution.py:39
  177.2 5.9 %collective-permute-start.13 = (bf16[256,256]{1,0:T(8,128)(2,1)S(1)}, bf16[256,256]{1,0:T(8,128)(2,1)S(1)}, u32[]{:S(2)}, u32[]{:S(2)}) collective-permute-start(bf16[256,256]{1,0:T(8,128)(2,1)S(1)} %get-tuple-element.18), channel_id=1, source_target_pairs={{0,384},{1,97},{2,386},{3,99},{4,388},{5,101},{6,390},{7,103},{8,3... | collective-permute-start | bytes 393224 | tf_op jit(solution)/shard_map/ppermute | solution.py:39
  179.6 50.7 %copy-start.19 = (bf16[256]{0:T(256)(128)(2,1)S(1)}, bf16[256]{0:T(256)(128)(2,1)}, u32[]{:S(2)}) copy-start(bf16[256]{0:T(256)(128)(2,1)} %param.18) | copy-start | bytes 1540
  184.4 38.5 %all-to-all-start.3 = ((bf16[32,32,256]{2,1,0:T(8,128)(2,1)}), bf16[32,32,256]{2,1,0:T(8,128)(2,1)S(1)}, u32[]{:S(2)}, u32[]{:S(2)}) async-start(bf16[32,32,256]{2,1,0:T(8,128)(2,1)} %bitcast.13), calls=%async_computation.3 | async-start | bytes 1048576 | tf_op jit(solution)/shard_map/all_to_all | solution.py:342
  224.1 12.7 %all-to-all-start.4 = ((f32[16,1,256]{2,1,0:T(1,128)}), f32[16,1,256]{2,1,0:T(1,128)S(1)}, u32[]{:S(2)}, u32[]{:S(2)}) async-start(f32[16,1,256]{2,1,0:T(1,128)} %get-tuple-element.20), calls=%async_computation.4 | async-start | bytes 32768 | tf_op jit(solution)/shard_map/all_to_all | solution.py:360
